TPU v7x, 128 devices: a 2x2x16 block of a 8x8x16 slice. The times are simulated.
128 devices in a mesh: grp: 4 (over y, x), ep: 32 (over z, core).
Axes of the slice: x: 2, y: 2, z: 16, core: 2. Of those that a mesh axis runs over, the one named last changes fastest.
The devices are a block of a 8x8x16 slice.
Arguments:
- tokens: bfloat16 [512, 2048], P(('grp', 'ep')), parts along dimension 0, may hold values from -6 to 6
- memory_state: float32 [512, 4, 256, 512], P(('grp', 'ep')), parts along dimension 0, may hold values from -0.6 to 0.6
- max_state: float32 [512, 4], P(('grp', 'ep')), parts along dimension 0, may hold values from -4 to 4
- norm_gain: float32 [2048], replicated, may hold values from 0.1 to 1.9
- query_weight: bfloat16 [2048, 1024], P(None, 'ep'), may hold values from -0.125 to 0.125
- key_weight: bfloat16 [2048, 1024], P(None, 'ep'), may hold values from -0.125 to 0.125
- value_weight: bfloat16 [2048, 2048], P(None, 'ep'), may hold values from -0.125 to 0.125
- output_gate: bfloat16 [2048, 2048], P(None, 'ep'), may hold values from -0.125 to 0.125
- input_gate: bfloat16 [2048, 4], replicated, may hold values from -0.125 to 0.125
- forget_gate: bfloat16 [2048, 4], replicated, may hold values from -0.125 to 0.125
- forget_bias: float32 [4], replicated, may hold values from -2 to 4
- head_gain: float32 [2048], replicated, may hold values from 0.1 to 1.9
- output_weight: bfloat16 [2048, 2048], P(None, 'ep'), may hold values from -0.125 to 0.125
- expert_norm: float32 [2048], replicated, may hold values from 0.1 to 1.9
- routed_experts: int32 [512, 4], P(('grp', 'ep')), parts along dimension 0, may hold values from 0 to 31, as said below
- route_weights: float32 [512, 4], P(('grp', 'ep')), parts along dimension 0, may hold values from 0.1 to 1
- expert_gate: bfloat16 [32, 2048, 512], P('ep'), may hold values from -0.125 to 0.125
- expert_lift: bfloat16 [32, 2048, 512], P('ep'), may hold values from -0.125 to 0.125
- expert_down: bfloat16 [32, 512, 2048], P('ep'), may hold values from -0.25 to 0.25
Outputs:
- layer_out: bfloat16 [512, 2048], P(('grp', 'ep')), parts along dimension 0
- new_memory: float32 [512, 4, 256, 512], P(('grp', 'ep')), parts along dimension 0
- new_max: float32 [512, 4], P(('grp', 'ep')), parts along dimension 0
There are 4 independent parts, one for each index of `grp`. A program takes and returns all parts, laid end to end along the dimension named above; an argument that names none is the same for every part. Nothing has to cross between parts.
Inputs may be any that keep to these rules, and one draw needn't show every extreme that they name: `routed_experts`: each row names 4 different experts of one group (expert e lies in group e // 8). No expert is named by more than 2 rows of one device, and some device has an expert named by 2 of its rows.
All inputs are finite; a program needn't handle non-finite values.
Results may differ from a plain program's by a relative error of at most 0.013.
Values may be sent and summed in bfloat16 or wider, within the bound.
No kernel may reach another device: no remote copies, remote signals or barrier semaphores. Data moves between devices by JAX's collectives and lax.ppermute only.
A program may use at most 64 MiB of HBM per device.

v0:
```python
import jax
import jax.numpy as jnp
from jax import lax
from jax.sharding import PartitionSpec as P

epsilon = 1e-06


def scaled_norm(entries, gain):
    return entries * lax.rsqrt(jnp.mean(entries * entries, axis=-1, keepdims=True) + epsilon) * gain


def expert_apply(blocks, gate_table, lift_table, down_table):
    gate_value = jnp.einsum(
        "secd,edf->secf", blocks, gate_table, preferred_element_type=jnp.float32
    )
    lift_value = jnp.einsum(
        "secd,edf->secf", blocks, lift_table, preferred_element_type=jnp.float32
    )
    hidden = (jax.nn.silu(gate_value) * lift_value).astype(jnp.bfloat16)
    return jnp.einsum(
        "secf,efd->secd", hidden, down_table, preferred_element_type=jnp.float32
    ).astype(jnp.bfloat16)


def body(
    tokens,
    memory_state,
    max_state,
    norm_gain,
    query_weight,
    key_weight,
    value_weight,
    output_gate,
    input_gate,
    forget_gate,
    forget_bias,
    head_gain,
    output_weight,
    expert_norm,
    routed_experts,
    route_weights,
    expert_gate,
    expert_lift,
    expert_down,
):
    seq_rows = tokens.shape[0]
    head_count = forget_bias.shape[0]
    key_size = memory_state.shape[2]
    value_size = memory_state.shape[3]
    axis_size = lax.axis_size("ep")
    inputs = tokens.astype(jnp.float32)
    normed = scaled_norm(inputs, norm_gain).astype(jnp.bfloat16)
    tables = (query_weight, key_weight, value_weight, output_gate)
    widths = [table.shape[1] for table in tables]
    piece = lax.all_gather(normed, "ep", axis=0, tiled=True)
    projected = jnp.concatenate(
        [
            jnp.dot(piece, table, preferred_element_type=jnp.float32).astype(jnp.bfloat16)
            for table in tables
        ],
        axis=1,
    )
    received = lax.all_to_all(projected, "ep", split_axis=0, concat_axis=1, tiled=True).reshape(
        seq_rows, axis_size, sum(widths)
    )
    pieces = []
    offset = 0
    for column_width in widths:
        pieces.append(
            received[:, :, offset : offset + column_width].reshape(
                seq_rows, axis_size * column_width
            )
        )
        offset = offset + column_width
    query_heads = pieces[0].astype(jnp.float32).reshape(seq_rows, head_count, key_size)
    key_heads = pieces[1].astype(jnp.float32).reshape(
        seq_rows, head_count, key_size
    ) * key_size ** (-0.5)
    value_heads = pieces[2].astype(jnp.float32).reshape(seq_rows, head_count, value_size)
    gate_heads = jax.nn.sigmoid(
        pieces[3].astype(jnp.float32).reshape(seq_rows, head_count, value_size)
    )
    input_logit = jnp.dot(normed, input_gate, preferred_element_type=jnp.float32)
    log_forget = jax.nn.log_sigmoid(
        jnp.dot(normed, forget_gate, preferred_element_type=jnp.float32) + forget_bias
    )
    new_max = jnp.maximum(log_forget + max_state, input_logit)
    carried = jnp.exp(log_forget + max_state - new_max)
    written = jnp.exp(input_logit - new_max)
    new_memory = (
        carried[:, :, None, None] * memory_state
        + (written[:, :, None] * key_heads)[:, :, :, None] * value_heads[:, :, None, :]
    )
    readout = jnp.einsum("shd,shde->she", query_heads, new_memory, precision=lax.Precision.HIGHEST)
    mixed = (
        (scaled_norm(readout, head_gain.reshape(head_count, value_size)) * gate_heads)
        .reshape(seq_rows, head_count * value_size)
        .astype(jnp.bfloat16)
    )
    columns = jnp.dot(
        lax.all_gather(mixed, "ep", axis=0, tiled=True),
        output_weight,
        preferred_element_type=jnp.float32,
    ).astype(jnp.bfloat16)
    branch = lax.all_to_all(columns, "ep", split_axis=0, concat_axis=1, tiled=True)
    residual = (inputs + branch.astype(jnp.float32)).astype(jnp.bfloat16)
    expert_in = scaled_norm(residual.astype(jnp.float32), expert_norm).astype(jnp.bfloat16)
    local_count = expert_gate.shape[0]
    expert_total = local_count * axis_size
    onehot = (
        routed_experts[:, :, None] == jnp.arange(expert_total, dtype=jnp.int32)[None, None, :]
    ).astype(jnp.int32)
    capacity = min(seq_rows, 2)
    present = jnp.sum(onehot, axis=1)
    before = jnp.cumsum(present, axis=0) - present
    slot_index = jnp.sum(onehot * before[:, None, :], axis=2)
    slot_match = (
        slot_index[:, :, None] == jnp.arange(capacity, dtype=jnp.int32)[None, None, :]
    ).astype(jnp.int32)
    placed = jnp.sum(onehot[:, :, :, None] * slot_match[:, :, None, :], axis=1).astype(jnp.bfloat16)
    send_buffer = (
        jnp.einsum("rec,rd->ecd", placed, expert_in, preferred_element_type=jnp.float32)
        .astype(jnp.bfloat16)
        .reshape(axis_size, local_count, capacity, expert_in.shape[1])
    )
    results = expert_apply(
        lax.all_to_all(send_buffer, "ep", split_axis=0, concat_axis=0, tiled=True),
        expert_gate,
        expert_lift,
        expert_down,
    )
    returned = lax.all_to_all(results, "ep", split_axis=0, concat_axis=0, tiled=True)
    flat_rows = returned.reshape(expert_total * capacity, expert_in.shape[1])
    picked = flat_rows[routed_experts * capacity + slot_index]
    weighted = lax.optimization_barrier(
        (route_weights[:, :, None] * picked.astype(jnp.float32)).astype(jnp.bfloat16)
    )
    expert_sum = jnp.sum(weighted.astype(jnp.float32), axis=1)
    layer_out = (residual.astype(jnp.float32) + expert_sum).astype(jnp.bfloat16)
    return (layer_out, new_memory, new_max)


def solution(mesh):
    return jax.shard_map(
        body,
        mesh=mesh,
        in_specs=(
            P(("grp", "ep"), None),
            P(("grp", "ep"), None, None, None),
            P(("grp", "ep"), None),
            P(),
            P(None, "ep"),
            P(None, "ep"),
            P(None, "ep"),
            P(None, "ep"),
            P(),
            P(),
            P(),
            P(),
            P(None, "ep"),
            P(),
            P(("grp", "ep"), None),
            P(("grp", "ep"), None),
            P("ep", None, None),
            P("ep", None, None),
            P("ep", None, None),
        ),
        out_specs=(
            P(("grp", "ep"), None),
            P(("grp", "ep"), None, None, None),
            P(("grp", "ep"), None),
        ),
        check_vma=False,
    )
```

profile of v0, /device:TPU:69, one launch (start us, length us, event | category | flops | bytes accessed | tf_op | source)
XLA Modules:
  0.0 182.9 jit_solution(4576648681838635549)
XLA Ops:
  0.7 1.0 fusion.37
  1.7 0.8 fusion.78
  2.5 42.0 %all-gather = bf16[32,4,2048]{2,1,0:T(4,128)(2,1)S(1)} all-gather(bf16[1,4,2048]{2,1,0:T(4,128)(2,1)S(1)} %fusion.78), channel_id=1, replica_groups=mesh['grp'=4,'ep'=32] {'ep'}, dimensions={0}, use_global_device_ids=true | all-gather | bytes 540672 | tf_op jit(solution)/shard_map/all_gather | solution.py:56
  44.5 0.1 reshape.151
  44.8 1.2 convolution_convert_fusion.3
  46.0 0.3 convolution_convert_fusion.4
  46.3 0.3 convolution_convert_fusion.5
  46.6 0.3 convolution_convert_fusion.6
  46.9 0.1 copy.67
  47.1 0.7 all_to_all.28
  47.7 6.0 %all-to-all-start = ((bf16[32,4,192]{2,1,0:T(4,128)(2,1)}), bf16[32,4,192]{2,1,0:T(4,128)(2,1)S(1)}, u32[]{:S(2)}, u32[]{:S(2)}) async-start(bf16[32,4,192]{2,1,0:T(4,128)(2,1)} %all_to_all.28), calls=%async_computation | async-start | bytes 131072 | tf_op jit(solution)/shard_map/all_to_all | solution.py:64
  53.8 0.1 fusion.57
  54.0 0.1 fusion.60
  54.1 0.1 subtract_exponential_fusion
  54.4 0.2 select_reduce_fusion
  54.6 11.9 %all-to-all-done = bf16[32,4,192]{2,1,0:T(4,128)(2,1)S(1)} async-done(((bf16[32,4,192]{2,1,0:T(4,128)(2,1)}), bf16[32,4,192]{2,1,0:T(4,128)(2,1)S(1)}, u32[]{:S(2)}, u32[]{:S(2)}) %all-to-all-start) | async-done | bytes 49184 | tf_op jit(solution)/shard_map/all_to_all | solution.py:64
  66.7 0.1 reshape.134
  66.8 0.1 reshape.135
  66.9 0.1 reshape.162
  67.0 4.0 %multiply_add_fusion = f32[4,4,256,512]{3,2,1,0:T(8,128)S(1)} fusion(f32[4,4,256,512]{3,2,1,0:T(8,128)} %param.20, f32[4,4,512]{2,1,0:T(4,128)S(1)} %reshape.135, f32[4,4,256]{2,1,0:T(4,128)S(1)} %broadcast_multiply_fusion, f32[4,4]{1,0:T(4,128)S(1)} %get-tuple-element.5), kind=kLoop, calls=%fused_computation.1 | loop fusion | flops 6291456 | bytes 16826432 | tf_op jit(solution)/shard_map/add | solution.py:92
  71.1 2.9 %fusion.61 = f32[4,4,1,512]{3,2,1,0:T(1,128)S(1)} fusion(bf16[4,4,256,1]{2,3,1,0:T(2,128)(2,1)S(1)} %reshape.162, f32[4,4,256,512]{3,2,1,0:T(8,128)S(1)} %multiply_add_fusion), kind=kOutput, calls=%fused_computation.84 | convolution fusion | flops 25165824 | bytes 8429568 | tf_op jit(solution)/shard_map/shd,shde->she/dot_general | solution.py:95
  74.0 0.5 copy-done.1
  74.5 0.1 fusion.45
  74.6 0.1 reshape.137
  74.8 30.0 %all-gather.1 = bf16[32,4,2048]{2,1,0:T(4,128)(2,1)S(1)} all-gather(bf16[1,4,2048]{2,1,0:T(4,128)(2,1)S(1)} %reshape.152), channel_id=1, replica_groups=mesh['grp'=4,'ep'=32] {'ep'}, dimensions={0}, use_global_device_ids=true | all-gather | bytes 540672 | tf_op jit(solution)/shard_map/all_gather | solution.py:102
  104.8 0.1 reshape.153
  104.9 0.3 convolution_convert_fusion.2
  105.3 0.1 copy.69
  105.4 0.7 reshape.163
  106.1 5.3 %all-to-all-start.1 = ((bf16[32,2,128]{2,1,0:T(2,128)(2,1)}), bf16[32,2,128]{2,1,0:T(2,128)(2,1)S(1)}, u32[]{:S(2)}, u32[]{:S(2)}) async-start(bf16[32,2,128]{2,1,0:T(2,128)(2,1)} %reshape.163), calls=%async_computation.1 | async-start | bytes 32768 | tf_op jit(solution)/shard_map/all_to_all | solution.py:106
  111.4 0.1 multiply_reduce_fusion
  111.5 11.4 %all-to-all-done.1 = bf16[32,2,128]{2,1,0:T(2,128)(2,1)S(1)} async-done(((bf16[32,2,128]{2,1,0:T(2,128)(2,1)}), bf16[32,2,128]{2,1,0:T(2,128)(2,1)S(1)}, u32[]{:S(2)}, u32[]{:S(2)}) %all-to-all-start.1) | async-done | bytes 16416 | tf_op jit(solution)/shard_map/all_to_all | solution.py:106
  123.0 0.1 reshape.138
  123.1 0.1 fusion.41
  123.3 0.3 fusion
  123.6 0.3 copy.72
  123.8 25.2 %all_to_all.39 = bf16[32,1,2,2048]{3,2,1,0:T(2,128)(2,1)S(1)} all-to-all(bf16[32,1,2,2048]{3,2,1,0:T(2,128)(2,1)S(1)} %copy.72), channel_id=1, replica_groups=mesh['grp'=4,'ep'=32] {'ep'}, dimensions={0} | all-to-all | bytes 524288 | tf_op jit(solution)/shard_map/all_to_all | solution.py:128
  149.1 2.0 %fusion.7 = f32[32,1,2,512]{3,0,2,1:T(8,128)S(1)} fusion(bf16[1,2048,512]{2,1,0:T(8,128)(2,1)} %param.35, bf16[32,1,2,2048]{3,2,1,0:T(2,128)(2,1)S(1)} %all_to_all.39), kind=kOutput, calls=%fused_computation.11 | convolution fusion | flops 134217728 | bytes 2490368 | tf_op jit(solution)/shard_map/secd,edf->secf/dot_general | solution.py:14
  151.1 2.5 %fusion.1 = bf16[32,1,2,2048]{3,0,2,1:T(8,128)(2,1)S(1)} fusion(bf16[1,512,2048]{2,1,0:T(8,128)(2,1)S(1)} %copy-done, bf16[1,2048,512]{2,1,0:T(8,128)(2,1)} %param.36, bf16[32,1,2,2048]{3,2,1,0:T(2,128)(2,1)S(1)} %all_to_all.39, f32[32,1,2,512]{3,0,2,1:T(8,128)S(1)} %fusion.7), kind=kOutput, calls=%fused_computation.5 | convolution fusion | flops 268763136 | bytes 4849664 | tf_op jit(solution)/shard_map/secf,efd->secd/dot_general | solution.py:21
  153.6 1.0 copy.74
  154.6 5.3 %all-to-all-start.3 = ((bf16[32,1,2,2048]{3,2,1,0:T(2,128)(2,1)}), bf16[32,1,2,2048]{3,2,1,0:T(2,128)(2,1)S(1)}, u32[]{:S(2)}, u32[]{:S(2)}) async-start(bf16[32,1,2,2048]{3,2,1,0:T(2,128)(2,1)} %copy.74), calls=%async_computation.3 | async-start | bytes 524288 | tf_op jit(solution)/shard_map/all_to_all | solution.py:133
  159.9 0.1 reshape.141
  160.0 21.3 %all-to-all-done.3 = bf16[32,1,2,2048]{3,2,1,0:T(2,128)(2,1)S(1)} async-done(((bf16[32,1,2,2048]{3,2,1,0:T(2,128)(2,1)}), bf16[32,1,2,2048]{3,2,1,0:T(2,128)(2,1)S(1)}, u32[]{:S(2)}, u32[]{:S(2)}) %all-to-all-start.3) | async-done | bytes 262176 | tf_op jit(solution)/shard_map/all_to_all | solution.py:133
  181.3 0.1 reshape.133
  181.4 0.6 gather_fusion
  182.1 0.1 multiply_convert_fusion
  182.2 0.1 convert_reduce_fusion
  182.3 0.6 fusion.44
  (64 shorter events, 0.9 us)
Async XLA Ops:
  0.6 150.5 %copy-start = (bf16[1,512,2048]{2,1,0:T(8,128)(2,1)S(1)}, bf16[1,512,2048]{2,1,0:T(8,128)(2,1)}, u32[]{:S(2)}) copy-start(bf16[1,512,2048]{2,1,0:T(8,128)(2,1)} %param.37) | copy-start | bytes 6291460
  0.6 45.4 %copy-start.2 = (bf16[2048,64]{0,1:T(8,128)(2,1)S(1)}, bf16[2048,64]{0,1:T(8,128)(2,1)}, u32[]{:S(2)}) copy-start(bf16[2048,64]{0,1:T(8,128)(2,1)} %param.25) | copy-start | bytes 786436
  0.7 45.7 %copy-start.5 = (bf16[2048,32]{0,1:T(8,128)(2,1)S(1)}, bf16[2048,32]{0,1:T(8,128)(2,1)}, u32[]{:S(2)}) copy-start(bf16[2048,32]{0,1:T(8,128)(2,1)} %param.24) | copy-start | bytes 393220
  1.7 0.8 copy-start.14
  44.5 9.2 %copy-start.4 = (bf16[4,2048]{1,0:T(4,128)(2,1)S(1)}, bf16[4,2048]{1,0:T(4,128)(2,1)}, u32[]{:S(2)}) copy-start(bf16[4,2048]{1,0:T(4,128)(2,1)} %param.19) | copy-start | bytes 49156
  44.7 2.0 %copy-start.6 = (bf16[2048,32]{0,1:T(8,128)(2,1)S(1)}, bf16[2048,32]{0,1:T(8,128)(2,1)}, u32[]{:S(2)}) copy-start(bf16[2048,32]{0,1:T(8,128)(2,1)} %param.23) | copy-start | bytes 393220
  44.7 9.0 %copy-start.9 = (f32[2048]{0:T(1024)S(1)}, f32[2048]{0:T(1024)}, u32[]{:S(2)}) copy-start(f32[2048]{0:T(1024)} %param.22) | copy-start | bytes 24580
  44.7 9.0 %copy-start.15 = (f32[4]{0:T(128)S(1)}, f32[4]{0:T(128)}, u32[]{:S(2)}) copy-start(f32[4]{0:T(128)} %copy-done.14) | copy-start | bytes 52
  44.7 9.1 %copy-start.7 = (s32[4,4]{1,0:T(4,128)S(1)}, s32[4,4]{1,0:T(4,128)}, u32[]{:S(2)}) copy-start(s32[4,4]{1,0:T(4,128)} %param.33) | copy-start | bytes 196
  44.7 9.3 %copy-start.16 = (bf16[2048,4]{0,1:T(4,128)(2,1)S(1)}, bf16[2048,4]{0,1:T(4,128)(2,1)}, u32[]{:S(2)}) copy-start(bf16[2048,4]{0,1:T(4,128)(2,1)} %param.27) | copy-start | bytes 49156
  44.7 9.4 %copy-start.17 = (bf16[2048,4]{0,1:T(4,128)(2,1)S(1)}, bf16[2048,4]{0,1:T(4,128)(2,1)}, u32[]{:S(2)}) copy-start(bf16[2048,4]{0,1:T(4,128)(2,1)} %param.28) | copy-start | bytes 49156
  44.7 9.4 %copy-start.18 = (f32[4,4]{1,0:T(4,128)S(1)}, f32[4,4]{1,0:T(4,128)}, u32[]{:S(2)}) copy-start(f32[4,4]{1,0:T(4,128)} %param.21) | copy-start | bytes 196
  44.7 9.4 %copy-start.19 = (f32[4]{0:T(128)S(1)}, f32[4]{0:T(128)}, u32[]{:S(2)}) copy-start(f32[4]{0:T(128)} %param.29) | copy-start | bytes 52
  44.8 9.5 %copy-start.11 = (f32[2048]{0:T(1024)S(1)}, f32[2048]{0:T(1024)}, u32[]{:S(2)}) copy-start(f32[2048]{0:T(1024)} %param.30) | copy-start | bytes 24580
  47.7 18.8 %all-to-all-start = ((bf16[32,4,192]{2,1,0:T(4,128)(2,1)}), bf16[32,4,192]{2,1,0:T(4,128)(2,1)S(1)}, u32[]{:S(2)}, u32[]{:S(2)}) async-start(bf16[32,4,192]{2,1,0:T(4,128)(2,1)} %all_to_all.28), calls=%async_computation | async-start | bytes 131072 | tf_op jit(solution)/shard_map/all_to_all | solution.py:64
  54.3 16.8 %copy-start.13 = (f32[4,4]{1,0:T(4,128)}, f32[4,4]{1,0:T(4,128)S(1)}, u32[]{:S(2)}) copy-start(f32[4,4]{1,0:T(4,128)S(1)} %get-tuple-element.6) | copy-start | bytes 196
  71.1 3.4 %copy-start.1 = (f32[4,4,256,512]{3,2,1,0:T(8,128)}, f32[4,4,256,512]{3,2,1,0:T(8,128)S(1)}, u32[]{:S(2)}) copy-start(f32[4,4,256,512]{3,2,1,0:T(8,128)S(1)} %multiply_add_fusion) | copy-start | bytes 25165828
  71.1 33.8 %copy-start.3 = (bf16[2048,64]{0,1:T(8,128)(2,1)S(1)}, bf16[2048,64]{0,1:T(8,128)(2,1)}, u32[]{:S(2)}) copy-start(bf16[2048,64]{0,1:T(8,128)(2,1)} %param.31) | copy-start | bytes 786436
  74.5 48.8 %copy-start.10 = (f32[2048]{0:T(1024)S(1)}, f32[2048]{0:T(1024)}, u32[]{:S(2)}) copy-start(f32[2048]{0:T(1024)} %param.32) | copy-start | bytes 24580
  106.1 16.8 %all-to-all-start.1 = ((bf16[32,2,128]{2,1,0:T(2,128)(2,1)}), bf16[32,2,128]{2,1,0:T(2,128)(2,1)S(1)}, u32[]{:S(2)}, u32[]{:S(2)}) async-start(bf16[32,2,128]{2,1,0:T(2,128)(2,1)} %reshape.163), calls=%async_computation.1 | async-start | bytes 32768 | tf_op jit(solution)/shard_map/all_to_all | solution.py:106
  151.1 8.8 %copy-start.8 = (s32[4,4]{1,0:T(4,128)S(1)}, s32[4,4]{1,0:T(4,128)}, u32[]{:S(2)}) copy-start(s32[4,4]{1,0:T(4,128)} %param.33) | copy-start | bytes 196
  153.6 28.5 %copy-start.12 = (f32[4,4]{1,0:T(4,128)S(1)}, f32[4,4]{1,0:T(4,128)}, u32[]{:S(2)}) copy-start(f32[4,4]{1,0:T(4,128)} %param.34) | copy-start | bytes 196
  154.6 26.7 %all-to-all-start.3 = ((bf16[32,1,2,2048]{3,2,1,0:T(2,128)(2,1)}), bf16[32,1,2,2048]{3,2,1,0:T(2,128)(2,1)S(1)}, u32[]{:S(2)}, u32[]{:S(2)}) async-start(bf16[32,1,2,2048]{3,2,1,0:T(2,128)(2,1)} %copy.74), calls=%async_computation.3 | async-start | bytes 524288 | tf_op jit(solution)/shard_map/all_to_all | solution.py:133
where the time goes:
time: 184 us; the launch traced here: 183 us
  blocking collectives  97.3 us (53%)
  waiting for transfers between devices  44.6 us (24%)
  starting transfers between devices  16.6 us (9%)
  matrix products  10.3 us (6%)
  other arithmetic  7.9 us (4%)
  local copies, waits for them, and re-layouts  5.07 us (3%)
    all_gather x1, blocking collectives, body(): piece = lax.all_gather(normed, 'ep', axis=0, tiled=True)  42 us
    all_gather x1, blocking collectives, body(): lax.all_gather(mixed, 'ep', axis=0, tiled=True)  30 us
    all_to_all x1, blocking collectives, body(): lax.all_to_all(send_buffer, 'ep', split_axis=0, concat_axis=0, tiled=True)  25.2 us
    all_to_all x1, waiting for transfers between devices, body(): lax.all_to_all(results, 'ep', split_axis=0, concat_axis=0, tiled=True)  21.3 us
    all_to_all x1, waiting for transfers between devices, body(): lax.all_to_all(projected, 'ep', split_axis=0, concat_axis=1, tiled=True)  11.9 us
    all_to_all x1, waiting for transfers between devices, body(): lax.all_to_all(columns, 'ep', split_axis=0, concat_axis=1, tiled=True)  11.4 us
    all_to_all x1, starting transfers between devices, body(): lax.all_to_all(projected, 'ep', split_axis=0, concat_axis=1, tiled=True)  5.98 us
    all_to_all x1, starting transfers between devices, body(): lax.all_to_all(columns, 'ep', split_axis=0, concat_axis=1, tiled=True)  5.33 us
  transfers between devices with their start and end apart: 3, of which 3 were waited for; matrix products, arithmetic and copies ran while one was open for 1% of the time, Pallas kernels for 0%

commit v1 on v0

v1 whole, which is shorter than its diff:
```python
import jax
import jax.numpy as jnp
from jax import lax
from jax.sharding import PartitionSpec as P

epsilon = 1e-06


def scaled_norm(entries, gain):
    return entries * lax.rsqrt(jnp.mean(entries * entries, axis=-1, keepdims=True) + epsilon) * gain


def gather_blocks(block):
    size = lax.axis_size("ep")
    chips = size // 2
    core = lax.axis_index("ep") % 2
    same = lax.all_to_all(
        jnp.broadcast_to(block[None], (chips,) + block.shape),
        "ep",
        split_axis=0,
        concat_axis=0,
        tiled=True,
        axis_index_groups=[list(range(0, size, 2)), list(range(1, size, 2))],
    )
    other = lax.ppermute(same, "ep", [(i, i ^ 1) for i in range(size)])
    first = jnp.where(core == 0, same, other)
    second = jnp.where(core == 0, other, same)
    return jnp.stack([first, second], axis=1)


def body(
    tokens,
    memory_state,
    max_state,
    norm_gain,
    query_weight,
    key_weight,
    value_weight,
    output_gate,
    input_gate,
    forget_gate,
    forget_bias,
    head_gain,
    output_weight,
    expert_norm,
    routed_experts,
    route_weights,
    expert_gate,
    expert_lift,
    expert_down,
):
    seq_rows, width = tokens.shape
    head_count = forget_bias.shape[0]
    key_size = memory_state.shape[2]
    value_size = memory_state.shape[3]
    axis_size = lax.axis_size("ep")
    me = lax.axis_index("ep")
    all_rows = axis_size * seq_rows
    capacity = min(seq_rows, 2)
    f32, bf16 = jnp.float32, jnp.bfloat16

    token_rows = gather_blocks(tokens).reshape(all_rows, width)
    normed_rows = scaled_norm(token_rows.astype(f32), norm_gain).astype(bf16)
    tables = (query_weight, key_weight, value_weight, output_gate)
    widths = [table.shape[1] for table in tables]
    total = sum(widths)
    projected = jnp.concatenate(
        [jnp.dot(normed_rows, table, preferred_element_type=f32).astype(bf16) for table in tables],
        axis=1,
    ).reshape(axis_size, seq_rows, total)
    choices = routed_experts.shape[1]
    routing = jnp.broadcast_to(
        jnp.pad(routed_experts.astype(bf16), ((0, 0), (0, 64 - choices)))[None],
        (axis_size, seq_rows, 64),
    )
    received = lax.all_to_all(
        jnp.concatenate([projected, routing], axis=2), "ep", split_axis=0, concat_axis=0, tiled=True
    )
    pieces = []
    offset = 0
    for column_width in widths:
        pieces.append(
            received[:, :, offset : offset + column_width]
            .transpose(1, 0, 2)
            .reshape(seq_rows, axis_size * column_width)
        )
        offset = offset + column_width
    routed_all = received[:, :, offset : offset + choices].astype(jnp.int32).reshape(all_rows, choices)

    inputs = tokens.astype(f32)
    normed = scaled_norm(inputs, norm_gain).astype(bf16)
    query_heads = pieces[0].astype(f32).reshape(seq_rows, head_count, key_size)
    key_heads = pieces[1].astype(f32).reshape(seq_rows, head_count, key_size) * key_size ** (-0.5)
    value_heads = pieces[2].astype(f32).reshape(seq_rows, head_count, value_size)
    gate_heads = jax.nn.sigmoid(pieces[3].astype(f32).reshape(seq_rows, head_count, value_size))
    input_logit = jnp.dot(normed, input_gate, preferred_element_type=f32)
    log_forget = jax.nn.log_sigmoid(
        jnp.dot(normed, forget_gate, preferred_element_type=f32) + forget_bias
    )
    new_max = jnp.maximum(log_forget + max_state, input_logit)
    carried = jnp.exp(log_forget + max_state - new_max)
    written = jnp.exp(input_logit - new_max)
    new_memory = (
        carried[:, :, None, None] * memory_state
        + (written[:, :, None] * key_heads)[:, :, :, None] * value_heads[:, :, None, :]
    )
    readout = jnp.einsum("shd,shde->she", query_heads, new_memory, precision=lax.Precision.HIGHEST)
    mixed = (
        (scaled_norm(readout, head_gain.reshape(head_count, value_size)) * gate_heads)
        .reshape(seq_rows, width)
        .astype(bf16)
    )
    mixed_rows = gather_blocks(mixed).reshape(all_rows, width)
    columns = lax.dot_general(
        output_weight, mixed_rows, (((0,), (1,)), ((), ())), preferred_element_type=f32
    ).astype(bf16)
    branch_columns = gather_blocks(columns).reshape(width, all_rows)

    named = jnp.any(routed_all == me, axis=1).reshape(axis_size, seq_rows).astype(jnp.int32)
    slot = jnp.cumsum(named, axis=1) - named
    place = (jnp.arange(axis_size)[:, None] * capacity + slot).reshape(all_rows)
    wanted = jnp.where(named.reshape(all_rows) > 0, place, -1)
    slots = axis_size * capacity
    pick = (wanted[None, :] == jnp.arange(slots)[:, None])
    own = (me * seq_rows + jnp.arange(seq_rows))[:, None] == jnp.arange(all_rows)[None, :]
    pick = jnp.concatenate([pick, own], axis=0).astype(bf16)
    branch = lax.dot_general(
        pick, branch_columns, (((1,), (1,)), ((), ())), preferred_element_type=f32
    )
    picked_tokens = jnp.dot(pick, token_rows, preferred_element_type=f32)
    residual = (picked_tokens + branch).astype(bf16)
    own_residual = residual[slots:]
    expert_in = scaled_norm(residual[:slots].astype(f32), expert_norm).astype(bf16)
    hidden = (
        jax.nn.silu(jnp.dot(expert_in, expert_gate[0], preferred_element_type=f32))
        * jnp.dot(expert_in, expert_lift[0], preferred_element_type=f32)
    ).astype(bf16)
    results = (
        jnp.dot(hidden, expert_down[0], preferred_element_type=f32)
        .astype(bf16)
        .reshape(axis_size, capacity, width)
    )
    returned = lax.all_to_all(results, "ep", split_axis=0, concat_axis=0, tiled=True)
    expert_ids = jnp.arange(axis_size, dtype=jnp.int32)
    chosen = (routed_experts[:, :, None] == expert_ids[None, None, :]).astype(jnp.int32)
    present = jnp.sum(chosen, axis=1)
    before = jnp.cumsum(present, axis=0) - present
    slot_index = jnp.sum(chosen * before[:, None, :], axis=2)
    picked = returned.reshape(slots, width)[routed_experts * capacity + slot_index]
    weighted = lax.optimization_barrier(
        (route_weights[:, :, None] * picked.astype(f32)).astype(bf16)
    )
    expert_sum = jnp.sum(weighted.astype(f32), axis=1)
    layer_out = (own_residual.astype(f32) + expert_sum).astype(bf16)
    return (layer_out, new_memory, new_max)


def solution(mesh):
    return jax.shard_map(
        body,
        mesh=mesh,
        in_specs=(
            P(("grp", "ep"), None),
            P(("grp", "ep"), None, None, None),
            P(("grp", "ep"), None),
            P(),
            P(None, "ep"),
            P(None, "ep"),
            P(None, "ep"),
            P(None, "ep"),
            P(),
            P(),
            P(),
            P(),
            P(None, "ep"),
            P(),
            P(("grp", "ep"), None),
            P(("grp", "ep"), None),
            P("ep", None, None),
            P("ep", None, None),
            P("ep", None, None),
        ),
        out_specs=(
            P(("grp", "ep"), None),
            P(("grp", "ep"), None, None, None),
            P(("grp", "ep"), None),
        ),
        check_vma=False,
    )
```

time: 184 us -> 162 us (0.88)
  blocking collectives: 97.3 us -> 15.5 us
  starting transfers between devices: 16.6 us -> 53.2 us
  waiting for transfers between devices: 44.6 us -> 59.5 us
  other arithmetic: 7.9 us -> 12.8 us
  matrix products: 10.3 us -> 12.2 us
  local copies, waits for them, and re-layouts: 5.07 us -> 6.92 us
    all_gather x2 -> x0, blocking collectives: 72 us -> none  [the longest x1 42 us: body(): piece = lax.all_gather(normed, 'ep', axis=0, tiled=True)]
    all_to_all x2 -> x3, starting transfers between devices: 11.3 us -> 29.1 us  [the longest x2 22.8 us: gather_blocks(): lax.all_to_all(jnp.broadcast_to(block[None], (chips,) + block.shape), 'ep...]
    ppermute x0 -> x3, starting transfers between devices: none -> 17.6 us  [gather_blocks(): other = lax.ppermute(same, 'ep', [(i, i ^ 1) for i in range(size)])]
    all_to_all x2 -> x3, waiting for transfers between devices: 23.3 us -> 35.4 us  [the longest x2 22.8 us: gather_blocks(): lax.all_to_all(jnp.broadcast_to(block[None], (chips,) + block.shape), 'ep...]
    all_to_all x1, blocking collectives: 25.2 us -> 15.5 us  [gather_blocks(): lax.all_to_all(jnp.broadcast_to(block[None], (chips,) + block.shape), 'ep...]
    broadcast_in_dim x1 -> x5, local copies, waits for them, and re-layouts: 0.08 us -> 2.6 us  [the longest x3 2.51 us: gather_blocks(): jnp.broadcast_to(block[None], (chips,) + block.shape)]
    ppermute x0 -> x3, waiting for transfers between devices: none -> 2.05 us  [gather_blocks(): other = lax.ppermute(same, 'ep', [(i, i ^ 1) for i in range(size)])]
    dot_general x10 -> x11, matrix products: 7.44 us -> 9.26 us  [the longest x4 3.31 us: body(): jnp.dot(normed_rows, table, preferred_element_type=f32).astype(bf16)]
  transfers between devices with their start and end apart: 3 -> 7, of which waited for: 3 -> 6; matrix products, arithmetic and copies ran while one was open for 1% -> 4% of each run, Pallas kernels for 0% -> 0%
where the time goes in v1:
time: 162 us; the launch traced here: 161 us
  waiting for transfers between devices  59.5 us (37%)
  starting transfers between devices  53.2 us (33%)
  blocking collectives  15.5 us (10%)
  other arithmetic  12.8 us (8%)
  matrix products  12.2 us (8%)
  local copies, waits for them, and re-layouts  6.92 us (4%)
    all_to_all x2, waiting for transfers between devices, gather_blocks(): lax.all_to_all(jnp.broadcast_to(block[None], (chips,) + block.shape), 'ep...  22.8 us
    all_to_all x2, starting transfers between devices, gather_blocks(): lax.all_to_all(jnp.broadcast_to(block[None], (chips,) + block.shape), 'ep...  22.8 us
    all_to_all x1, waiting for transfers between devices, body(): lax.all_to_all(results, 'ep', split_axis=0, concat_axis=0, tiled=True)  22 us
    ppermute x3, starting transfers between devices, gather_blocks(): other = lax.ppermute(same, 'ep', [(i, i ^ 1) for i in range(size)])  17.6 us
    all_to_all x1, blocking collectives, gather_blocks(): lax.all_to_all(jnp.broadcast_to(block[None], (chips,) + block.shape), 'ep...  15.5 us
    all_to_all x1, waiting for transfers between devices, body(): lax.all_to_all(jnp.concatenate([projected, routing], axis=2), 'ep', split...  12.6 us
    all_to_all x1, starting transfers between devices, body(): lax.all_to_all(results, 'ep', split_axis=0, concat_axis=0, tiled=True)  6.52 us
    all_to_all x1, starting transfers between devices, body(): lax.all_to_all(jnp.concatenate([projected, routing], axis=2), 'ep', split...  6.29 us
  transfers between devices with their start and end apart: 7, of which 6 were waited for; matrix products, arithmetic and copies ran while one was open for 4% of the time, Pallas kernels for 0%

profile of v1, /device:TPU:69, one launch (start us, length us, event | category | flops | bytes accessed | tf_op | source)
XLA Modules:
  0.0 161.2 jit_solution(2466545304188573726)
XLA Ops:
  0.6 1.7 %broadcast_in_dim.13 = bf16[16,4,2048]{2,1,0:T(4,128)(2,1)} broadcast(bf16[4,2048]{1,0:T(4,128)(2,1)} %param.19), dimensions={1,2} | broadcast | bytes 278528 | tf_op jit(solution)/shard_map/broadcast_in_dim | solution.py:18
  2.3 17.6 %all-to-all-start = ((bf16[16,4,2048]{2,1,0:T(4,128)(2,1)}), bf16[16,4,2048]{2,1,0:T(4,128)(2,1)S(1)}, u32[]{:S(2)}, u32[]{:S(2)}) async-start(bf16[16,4,2048]{2,1,0:T(4,128)(2,1)} %broadcast_in_dim.13), calls=%async_computation | async-start | bytes 524288 | tf_op jit(solution)/shard_map/all_to_all | solution.py:17
  19.9 0.8 convert_reduce_fusion.1
  20.7 0.8 fusion.29
  21.6 0.9 select_reduce_fusion
  22.5 0.8 fusion.31
  23.3 10.2 %all-to-all-done = bf16[16,4,2048]{2,1,0:T(4,128)(2,1)S(1)} async-done(((bf16[16,4,2048]{2,1,0:T(4,128)(2,1)}), bf16[16,4,2048]{2,1,0:T(4,128)(2,1)S(1)}, u32[]{:S(2)}, u32[]{:S(2)}) %all-to-all-start) | async-done | bytes 262176 | tf_op jit(solution)/shard_map/all_to_all | solution.py:17
  33.5 5.4 %collective-permute-start = (bf16[16,4,2048]{2,1,0:T(4,128)(2,1)S(1)}, bf16[16,4,2048]{2,1,0:T(4,128)(2,1)S(1)}, u32[]{:S(2)}, u32[]{:S(2)}) collective-permute-start(bf16[16,4,2048]{2,1,0:T(4,128)(2,1)S(1)} %all-to-all-done), channel_id=1, source_target_pairs={{0,1},{1,0},{2,3},{3,2},{4,5},{5,4},{6,7},{7,6},{8,9},{9,8},{10,11... | collective-permute-start | bytes 786440 | tf_op jit(solution)/shard_map/ppermute | solution.py:25
  38.9 0.8 compare_select_fusion
  39.7 0.8 fusion.43
  40.5 0.2 select_bitcast_fusion.5
  40.7 0.6 multiply_reduce_fusion
  41.4 0.2 copy.49
  41.9 1.3 convolution_convert_fusion.5
  43.2 1.3 convolution_convert_fusion.4
  44.5 0.4 convolution_convert_fusion.3
  44.9 0.4 convolution_convert_fusion.2
  45.4 0.7 pad_maximum_fusion.3
  46.2 6.3 %all-to-all-start.1 = ((bf16[32,4,256]{2,1,0:T(4,128)(2,1)}), bf16[32,4,256]{2,1,0:T(4,128)(2,1)S(1)}, u32[]{:S(2)}, u32[]{:S(2)}) async-start(bf16[32,4,256]{2,1,0:T(4,128)(2,1)} %pad_maximum_fusion.3), calls=%async_computation.1 | async-start | bytes 131072 | tf_op jit(solution)/shard_map/all_to_all | solution.py:76
  52.5 0.1 subtract_exponential_fusion
  52.7 12.6 %all-to-all-done.1 = bf16[32,4,256]{2,1,0:T(4,128)(2,1)S(1)} async-done(((bf16[32,4,256]{2,1,0:T(4,128)(2,1)}), bf16[32,4,256]{2,1,0:T(4,128)(2,1)S(1)}, u32[]{:S(2)}, u32[]{:S(2)}) %all-to-all-start.1) | async-done | bytes 65568 | tf_op jit(solution)/shard_map/all_to_all | solution.py:76
  65.8 4.0 %multiply_add_fusion = f32[4,4,256,512]{3,2,1,0:T(8,128)S(1)} fusion(f32[4,4,256,512]{3,2,1,0:T(8,128)} %param.20, f32[4,4,512]{2,1,0:T(4,128)S(1)} %reshape.174, f32[4,4,256]{2,1,0:T(4,128)S(1)} %broadcast_multiply_fusion, f32[4,4]{1,0:T(4,128)S(1)} %get-tuple-element.3), kind=kLoop, calls=%fused_computation.1 | loop fusion | flops 6291456 | bytes 16826432 | tf_op jit(solution)/shard_map/add | solution.py:104
  69.9 2.9 %fusion.44 = f32[4,4,1,512]{3,2,1,0:T(1,128)S(1)} fusion(bf16[4,4,256,1]{2,3,1,0:T(2,128)(2,1)S(1)} %reshape.191, f32[4,4,256,512]{3,2,1,0:T(8,128)S(1)} %multiply_add_fusion), kind=kOutput, calls=%fused_computation.91 | convolution fusion | flops 25165824 | bytes 8429568 | tf_op jit(solution)/shard_map/shd,shde->she/dot_general | solution.py:107
  72.8 0.5 copy-done.1
  73.8 15.5 %all_to_all.25 = bf16[16,4,2048]{2,1,0:T(4,128)(2,1)S(1)} all-to-all(bf16[16,4,2048]{2,1,0:T(4,128)(2,1)S(1)} %broadcast_in_dim.16), channel_id=1, replica_groups={{0,2,4,6,8,10,12,14,16,18,20,22,24,26,28,30},{1,3,5,7,9,11,13,15,17,19,..., dimensions={0} | all-to-all | bytes 524288 | tf_op jit(solution)/shard_map/all_to_all | solution.py:17
  89.2 7.0 %collective-permute-start.1 = (bf16[16,4,2048]{2,1,0:T(4,128)(2,1)S(1)}, bf16[16,4,2048]{2,1,0:T(4,128)(2,1)S(1)}, u32[]{:S(2)}, u32[]{:S(2)}) collective-permute-start(bf16[16,4,2048]{2,1,0:T(4,128)(2,1)S(1)} %all_to_all.25), channel_id=1, source_target_pairs={{0,1},{1,0},{2,3},{3,2},{4,5},{5,4},{6,7},{7,6},{8,9},{9,8},{10,11... | collective-permute-start | bytes 786440 | tf_op jit(solution)/shard_map/ppermute | solution.py:25
  96.2 1.2 collective-permute-done.1
  97.4 0.2 select_bitcast_fusion.3
  97.6 0.3 pad_maximum_fusion.1
  97.9 0.9 reshape.169
  98.9 1.3 fusion.14
  100.2 0.7 broadcast_in_dim.17
  100.9 5.3 %all-to-all-start.3 = ((bf16[16,64,128]{2,1,0:T(8,128)(2,1)}), bf16[16,64,128]{2,1,0:T(8,128)(2,1)S(1)}, u32[]{:S(2)}, u32[]{:S(2)}) async-start(bf16[16,64,128]{2,1,0:T(8,128)(2,1)} %broadcast_in_dim.17), calls=%async_computation.3 | async-start | bytes 524288 | tf_op jit(solution)/shard_map/all_to_all | solution.py:17
  106.3 0.7 fusion.25
  107.0 0.2 reduce_window_sum.22
  107.4 12.7 %all-to-all-done.3 = bf16[16,64,128]{2,1,0:T(8,128)(2,1)S(1)} async-done(((bf16[16,64,128]{2,1,0:T(8,128)(2,1)}), bf16[16,64,128]{2,1,0:T(8,128)(2,1)S(1)}, u32[]{:S(2)}, u32[]{:S(2)}) %all-to-all-start.3) | async-done | bytes 262176 | tf_op jit(solution)/shard_map/all_to_all | solution.py:17
  120.0 5.1 %collective-permute-start.2 = (bf16[16,64,128]{2,1,0:T(8,128)(2,1)S(1)}, bf16[16,64,128]{2,1,0:T(8,128)(2,1)S(1)}, u32[]{:S(2)}, u32[]{:S(2)}) collective-permute-start(bf16[16,64,128]{2,1,0:T(8,128)(2,1)S(1)} %all-to-all-done.3), channel_id=1, source_target_pairs={{0,1},{1,0},{2,3},{3,2},{4,5},{5,4},{6,7},{7,6},{8,9},{9,8},{10,11... | collective-permute-start | bytes 786440 | tf_op jit(solution)/shard_map/ppermute | solution.py:25
  125.2 0.2 fusion.37
  125.4 0.9 collective-permute-done.2
  126.4 0.3 fusion
  126.7 0.2 fusion.16
  127.0 0.5 fusion.4
  127.5 2.6 %convolution_convert_fusion = bf16[64,2048]{1,0:T(8,128)(2,1)S(1)} fusion(bf16[1,512,2048]{2,1,0:T(8,128)(2,1)S(1)} %copy-done, bf16[1,2048,512]{2,1,0:T(8,128)(2,1)} %param.36, f32[64,512]{1,0:T(8,128)S(1)} %fusion.4, f32[2048]{0:T(1024)S(1)} %copy-done.4, f32[64]{0:T(128)S(1)} %add_rsqrt_fusion.2, bf16[68,2048]{1,0:T(8,128)(2,1)S(1)} %fusion), kind=kOutput, calls=%fused_computation.4 | convolution fusion | flops 269287424 | bytes 4858368 | tf_op jit(solution)/shard_map/dot_general | solution.py:139
  130.1 0.9 reshape.171
  131.0 6.5 %all-to-all-start.4 = ((bf16[32,2,2048]{2,1,0:T(2,128)(2,1)}), bf16[32,2,2048]{2,1,0:T(2,128)(2,1)S(1)}, u32[]{:S(2)}, u32[]{:S(2)}) async-start(bf16[32,2,2048]{2,1,0:T(2,128)(2,1)} %reshape.171), calls=%async_computation.4 | async-start | bytes 524288 | tf_op jit(solution)/shard_map/all_to_all | solution.py:143
  137.6 22.0 %all-to-all-done.4 = bf16[32,2,2048]{2,1,0:T(2,128)(2,1)S(1)} async-done(((bf16[32,2,2048]{2,1,0:T(2,128)(2,1)}), bf16[32,2,2048]{2,1,0:T(2,128)(2,1)S(1)}, u32[]{:S(2)}, u32[]{:S(2)}) %all-to-all-start.4) | async-done | bytes 262176 | tf_op jit(solution)/shard_map/all_to_all | solution.py:143
  159.7 0.6 gather_fusion
  160.6 0.6 add_convert_fusion
  (75 shorter events, 2.5 us)
Async XLA Ops:
  0.6 126.9 %copy-start = (bf16[1,512,2048]{2,1,0:T(8,128)(2,1)S(1)}, bf16[1,512,2048]{2,1,0:T(8,128)(2,1)}, u32[]{:S(2)}) copy-start(bf16[1,512,2048]{2,1,0:T(8,128)(2,1)} %param.37) | copy-start | bytes 6291460
  2.3 31.1 %all-to-all-start = ((bf16[16,4,2048]{2,1,0:T(4,128)(2,1)}), bf16[16,4,2048]{2,1,0:T(4,128)(2,1)S(1)}, u32[]{:S(2)}, u32[]{:S(2)}) async-start(bf16[16,4,2048]{2,1,0:T(4,128)(2,1)} %broadcast_in_dim.13), calls=%async_computation | async-start | bytes 524288 | tf_op jit(solution)/shard_map/all_to_all | solution.py:17
  33.5 7.1 %collective-permute-start = (bf16[16,4,2048]{2,1,0:T(4,128)(2,1)S(1)}, bf16[16,4,2048]{2,1,0:T(4,128)(2,1)S(1)}, u32[]{:S(2)}, u32[]{:S(2)}) collective-permute-start(bf16[16,4,2048]{2,1,0:T(4,128)(2,1)S(1)} %all-to-all-done), channel_id=1, source_target_pairs={{0,1},{1,0},{2,3},{3,2},{4,5},{5,4},{6,7},{7,6},{8,9},{9,8},{10,11... | collective-permute-start | bytes 786440 | tf_op jit(solution)/shard_map/ppermute | solution.py:25
  40.5 1.3 copy-start.6
  41.3 3.1 %copy-start.9 = (bf16[2048,64]{0,1:T(8,128)(2,1)S(1)}, bf16[2048,64]{0,1:T(8,128)(2,1)}, u32[]{:S(2)}) copy-start(bf16[2048,64]{0,1:T(8,128)(2,1)} %param.25) | copy-start | bytes 786436
  41.7 3.2 %copy-start.10 = (bf16[2048,64]{0,1:T(8,128)(2,1)S(1)}, bf16[2048,64]{0,1:T(8,128)(2,1)}, u32[]{:S(2)}) copy-start(bf16[2048,64]{0,1:T(8,128)(2,1)} %param.26) | copy-start | bytes 786436
  43.1 9.3 %copy-start.11 = (bf16[2048,4]{0,1:T(4,128)(2,1)S(1)}, bf16[2048,4]{0,1:T(4,128)(2,1)}, u32[]{:S(2)}) copy-start(bf16[2048,4]{0,1:T(4,128)(2,1)} %param.28) | copy-start | bytes 49156
  43.1 9.3 %copy-start.12 = (f32[4,4]{1,0:T(4,128)S(1)}, f32[4,4]{1,0:T(4,128)}, u32[]{:S(2)}) copy-start(f32[4,4]{1,0:T(4,128)} %param.21) | copy-start | bytes 196
  43.2 9.3 %copy-start.13 = (f32[4]{0:T(128)S(1)}, f32[4]{0:T(128)}, u32[]{:S(2)}) copy-start(f32[4]{0:T(128)} %param.29) | copy-start | bytes 52
  43.2 9.5 %copy-start.5 = (f32[2048]{0:T(1024)S(1)}, f32[2048]{0:T(1024)}, u32[]{:S(2)}) copy-start(f32[2048]{0:T(1024)} %param.30) | copy-start | bytes 24580
  46.2 19.1 %all-to-all-start.1 = ((bf16[32,4,256]{2,1,0:T(4,128)(2,1)}), bf16[32,4,256]{2,1,0:T(4,128)(2,1)S(1)}, u32[]{:S(2)}, u32[]{:S(2)}) async-start(bf16[32,4,256]{2,1,0:T(4,128)(2,1)} %pad_maximum_fusion.3), calls=%async_computation.1 | async-start | bytes 131072 | tf_op jit(solution)/shard_map/all_to_all | solution.py:76
  52.7 17.2 %copy-start.8 = (f32[4,4]{1,0:T(4,128)}, f32[4,4]{1,0:T(4,128)S(1)}, u32[]{:S(2)}) copy-start(f32[4,4]{1,0:T(4,128)S(1)} %get-tuple-element.4) | copy-start | bytes 196
  69.9 3.4 %copy-start.1 = (f32[4,4,256,512]{3,2,1,0:T(8,128)}, f32[4,4,256,512]{3,2,1,0:T(8,128)S(1)}, u32[]{:S(2)}) copy-start(f32[4,4,256,512]{3,2,1,0:T(8,128)S(1)} %multiply_add_fusion) | copy-start | bytes 25165828
  73.4 25.4 %copy-start.3 = (bf16[2048,64]{0,1:T(8,128)(2,1)S(1)}, bf16[2048,64]{0,1:T(8,128)(2,1)}, u32[]{:S(2)}) copy-start(bf16[2048,64]{0,1:T(8,128)(2,1)} %param.31) | copy-start | bytes 786436
  89.2 8.1 %collective-permute-start.1 = (bf16[16,4,2048]{2,1,0:T(4,128)(2,1)S(1)}, bf16[16,4,2048]{2,1,0:T(4,128)(2,1)S(1)}, u32[]{:S(2)}, u32[]{:S(2)}) collective-permute-start(bf16[16,4,2048]{2,1,0:T(4,128)(2,1)S(1)} %all_to_all.25), channel_id=1, source_target_pairs={{0,1},{1,0},{2,3},{3,2},{4,5},{5,4},{6,7},{7,6},{8,9},{9,8},{10,11... | collective-permute-start | bytes 786440 | tf_op jit(solution)/shard_map/ppermute | solution.py:25
  100.9 19.1 %all-to-all-start.3 = ((bf16[16,64,128]{2,1,0:T(8,128)(2,1)}), bf16[16,64,128]{2,1,0:T(8,128)(2,1)S(1)}, u32[]{:S(2)}, u32[]{:S(2)}) async-start(bf16[16,64,128]{2,1,0:T(8,128)(2,1)} %broadcast_in_dim.17), calls=%async_computation.3 | async-start | bytes 524288 | tf_op jit(solution)/shard_map/all_to_all | solution.py:17
  120.0 6.3 %collective-permute-start.2 = (bf16[16,64,128]{2,1,0:T(8,128)(2,1)S(1)}, bf16[16,64,128]{2,1,0:T(8,128)(2,1)S(1)}, u32[]{:S(2)}, u32[]{:S(2)}) collective-permute-start(bf16[16,64,128]{2,1,0:T(8,128)(2,1)S(1)} %all-to-all-done.3), channel_id=1, source_target_pairs={{0,1},{1,0},{2,3},{3,2},{4,5},{5,4},{6,7},{7,6},{8,9},{9,8},{10,11... | collective-permute-start | bytes 786440 | tf_op jit(solution)/shard_map/ppermute | solution.py:25
  125.4 1.6 copy-start.2
  125.4 1.6 copy-start.4
  130.1 30.3 %copy-start.7 = (f32[4,4]{1,0:T(4,128)S(1)}, f32[4,4]{1,0:T(4,128)}, u32[]{:S(2)}) copy-start(f32[4,4]{1,0:T(4,128)} %param.34) | copy-start | bytes 196
  131.0 28.6 %all-to-all-start.4 = ((bf16[32,2,2048]{2,1,0:T(2,128)(2,1)}), bf16[32,2,2048]{2,1,0:T(2,128)(2,1)S(1)}, u32[]{:S(2)}, u32[]{:S(2)}) async-start(bf16[32,2,2048]{2,1,0:T(2,128)(2,1)} %reshape.171), calls=%async_computation.4 | async-start | bytes 524288 | tf_op jit(solution)/shard_map/all_to_all | solution.py:143

commit v2 on v1

v2 whole, which is shorter than its diff:
```python
import jax
import jax.numpy as jnp
from jax import lax
from jax.experimental import pallas as pl
from jax.experimental.pallas import tpu as pltpu
from jax.sharding import PartitionSpec as P

epsilon = 1e-06
f32, bf16 = jnp.float32, jnp.bfloat16
lanes = 128
whole = pl.BlockSpec(memory_space=pltpu.VMEM)


def scaled_norm(entries, gain):
    return entries * lax.rsqrt(jnp.mean(entries * entries, axis=-1, keepdims=True) + epsilon) * gain


def exchange(blocks):
    size = lax.axis_size("ep")
    return lax.all_to_all(
        blocks,
        "ep",
        split_axis=0,
        concat_axis=0,
        tiled=True,
        axis_index_groups=[list(range(0, size, 2)), list(range(1, size, 2))],
    )


def spread(block):
    chips = lax.axis_size("ep") // 2
    return exchange(jnp.broadcast_to(block[None], (chips,) + block.shape))


def partner(block):
    return lax.ppermute(block, "ep", [(i, i ^ 1) for i in range(lax.axis_size("ep"))])


def project_kernel(rows, gain, table, out):
    entries = rows[...].astype(f32)
    normed = scaled_norm(entries, gain[...]).astype(bf16)
    out[...] = lax.dot_general(
        normed, table[...], (((1,), (1,)), ((), ())), preferred_element_type=f32
    ).astype(bf16)


def readout_kernel(chips, decayed, received, weight, gain, out, sums):
    seqs, heads, keys, values = decayed.shape
    per_head = chips // heads
    part = keys // per_head
    flat = received[...].astype(f32)
    pairs = flat[:, :lanes]
    columns = pairs.T
    for head in range(heads):
        for seq in range(seqs):
            total = jnp.zeros((8, values), f32)
            for j in range(per_head):
                at = (head * per_head + j) * seqs + seq
                block = decayed[seq, head, j * part : (j + 1) * part, :]
                terms = block * columns[:part, at : at + 1]
                total = total + jnp.sum(terms.reshape(part // 8, 8, values), axis=0)
            row = jnp.sum(total, axis=0, keepdims=True)
            for j in range(per_head):
                at = (head * per_head + j) * seqs + seq
                sums[at : at + 1, :] = row[:, j * lanes : (j + 1) * lanes]

    def head_total(entries):
        by_chip = entries.reshape(heads, per_head // 2, 2 * seqs, lanes)
        both = jnp.sum(by_chip, axis=1)
        both = both + jnp.concatenate([both[:, seqs:], both[:, :seqs]], axis=1)
        both = jnp.broadcast_to(both[:, None], by_chip.shape).reshape(entries.shape)
        return jnp.sum(both, axis=-1, keepdims=True)

    products = pairs * jnp.concatenate([pairs[:, part:], pairs[:, :part]], axis=1)
    match = head_total(products) * 0.5
    readout = sums[...] + (weight[...] * match) * flat[:, lanes : 2 * lanes]
    scale = lax.rsqrt(head_total(readout * readout) / values + epsilon)
    gates = jax.nn.sigmoid(flat[:, 2 * lanes : 3 * lanes])
    out[...] = (readout * scale * gain[...] * gates).astype(bf16)


def body(
    tokens,
    memory_state,
    max_state,
    norm_gain,
    query_weight,
    key_weight,
    value_weight,
    output_gate,
    input_gate,
    forget_gate,
    forget_bias,
    head_gain,
    output_weight,
    expert_norm,
    routed_experts,
    route_weights,
    expert_gate,
    expert_lift,
    expert_down,
):
    seq_rows, width = tokens.shape
    head_count = forget_bias.shape[0]
    key_size = memory_state.shape[2]
    value_size = memory_state.shape[3]
    axis_size = lax.axis_size("ep")
    chips = axis_size // 2
    me = lax.axis_index("ep")
    core = me % 2
    half_rows = chips * seq_rows
    capacity = min(seq_rows, 2)
    choices = routed_experts.shape[1]

    same_tokens = spread(tokens).reshape(half_rows, width)

    tables = []
    for table in (query_weight, key_weight, value_weight, output_gate, output_weight):
        mine = table.T
        theirs = partner(mine)
        tables.append(
            jnp.where(
                core == 0,
                jnp.concatenate([mine, theirs], axis=0),
                jnp.concatenate([theirs, mine], axis=0),
            )
        )
    table = jnp.concatenate(tables[:4], axis=0)
    total = table.shape[0]

    inputs = tokens.astype(f32)
    normed = scaled_norm(inputs, norm_gain).astype(bf16)
    input_logit = jnp.dot(normed, input_gate, preferred_element_type=f32)
    log_forget = jax.nn.log_sigmoid(
        jnp.dot(normed, forget_gate, preferred_element_type=f32) + forget_bias
    )
    new_max = jnp.maximum(log_forget + max_state, input_logit)
    carried = jnp.exp(log_forget + max_state - new_max)
    written = jnp.exp(input_logit - new_max) * key_size ** (-0.5)
    decayed = carried[:, :, None, None] * memory_state
    per_head = chips // head_count
    by_chip = (head_count, per_head, seq_rows, lanes)
    weight_rows = jnp.broadcast_to(written.T[:, None, :, None], by_chip).reshape(half_rows, lanes)
    gain_rows = jnp.broadcast_to(
        head_gain.reshape(head_count, per_head, 1, lanes), by_chip
    ).reshape(half_rows, lanes)
    same_tokens, table, decayed, weight_rows, gain_rows = lax.optimization_barrier(
        (same_tokens, table, decayed, weight_rows, gain_rows)
    )

    projected = pl.pallas_call(
        project_kernel,
        out_shape=jax.ShapeDtypeStruct((half_rows, total), bf16),
        in_specs=[whole] * 3,
        out_specs=whole,
        name="project",
    )(same_tokens, norm_gain[None], table)
    routing = jnp.pad(routed_experts.astype(bf16), ((0, 0), (0, lanes - choices)))
    received = exchange(
        jnp.concatenate(
            [
                projected.reshape(chips, seq_rows, total),
                jnp.broadcast_to(routing[None], (chips, seq_rows, lanes)),
            ],
            axis=2,
        )
    ).reshape(half_rows, total + lanes)

    mixed = pl.pallas_call(
        lambda *refs: readout_kernel(chips, *refs),
        out_shape=jax.ShapeDtypeStruct((half_rows, lanes), bf16),
        in_specs=[whole] * 4,
        out_specs=whole,
        scratch_shapes=[pltpu.VMEM((half_rows, lanes), f32)],
        compiler_params=pltpu.CompilerParams(vmem_limit_bytes=24 << 20),
        name="readout",
    )(decayed, received, weight_rows, gain_rows)
    mixed = mixed.reshape(chips, seq_rows, lanes).transpose(1, 0, 2).reshape(seq_rows, width)
    same_mixed = spread(mixed).reshape(half_rows, width)

    by_source = received.reshape(chips, seq_rows, total + lanes)
    edge = total // 6

    def own_columns(start, size):
        return (
            by_source[:, :, start : start + size]
            .transpose(1, 0, 2)
            .reshape(seq_rows, head_count, chips * size // head_count)
            .astype(f32)
        )

    key_heads = own_columns(edge, edge)
    value_heads = own_columns(2 * edge, 2 * edge)
    new_memory = (
        decayed + (written[:, :, None] * key_heads)[:, :, :, None] * value_heads[:, :, None, :]
    )

    columns = lax.dot_general(
        same_mixed, tables[4], (((1,), (1,)), ((), ())), preferred_element_type=f32
    ).astype(bf16)
    same_branch = spread(columns)
    other_branch = partner(same_branch)
    other_tokens = partner(same_tokens)

    same_routed = received[:, total : total + choices]
    other_routed = partner(received[:, total:])[:, :choices]
    same_named = jnp.any(same_routed == me.astype(bf16), axis=1).astype(jnp.int32)
    other_named = jnp.any(other_routed == me.astype(bf16), axis=1).astype(jnp.int32)
    named = jnp.stack([same_named, other_named]).reshape(2, chips, seq_rows)
    slot = jnp.cumsum(named, axis=2) - named
    source = 2 * jnp.arange(chips)[None, :, None] + jnp.stack([core, 1 - core])[:, None, None]
    place = jnp.where(named > 0, source * capacity + slot, -1).reshape(2 * half_rows)
    slots = axis_size * capacity
    pick = place[None, :] == jnp.arange(slots)[:, None]
    own = ((me // 2) * seq_rows + jnp.arange(seq_rows))[:, None] == jnp.arange(2 * half_rows)[None, :]
    pick = jnp.concatenate([pick, own], axis=0).astype(bf16)
    branch_rows = jnp.concatenate(
        [b.transpose(1, 0, 2).reshape(half_rows, width) for b in (same_branch, other_branch)], axis=0
    )
    token_rows = jnp.concatenate([same_tokens, other_tokens], axis=0)
    branch = jnp.dot(pick, branch_rows, preferred_element_type=f32)
    picked_tokens = jnp.dot(pick, token_rows, preferred_element_type=f32)
    residual = (picked_tokens + branch).astype(bf16)
    own_residual = residual[slots:]
    expert_in = scaled_norm(residual[:slots].astype(f32), expert_norm).astype(bf16)
    hidden = (
        jax.nn.silu(jnp.dot(expert_in, expert_gate[0], preferred_element_type=f32))
        * jnp.dot(expert_in, expert_lift[0], preferred_element_type=f32)
    ).astype(bf16)
    results = (
        jnp.dot(hidden, expert_down[0], preferred_element_type=f32)
        .astype(bf16)
        .reshape(axis_size, capacity, width)
    )
    returned = lax.all_to_all(results, "ep", split_axis=0, concat_axis=0, tiled=True)
    expert_ids = jnp.arange(axis_size, dtype=jnp.int32)
    chosen = (routed_experts[:, :, None] == expert_ids[None, None, :]).astype(jnp.int32)
    present = jnp.sum(chosen, axis=1)
    before = jnp.cumsum(present, axis=0) - present
    slot_index = jnp.sum(chosen * before[:, None, :], axis=2)
    picked = returned.reshape(slots, width)[routed_experts * capacity + slot_index]
    weighted = lax.optimization_barrier(
        (route_weights[:, :, None] * picked.astype(f32)).astype(bf16)
    )
    expert_sum = jnp.sum(weighted.astype(f32), axis=1)
    layer_out = (own_residual.astype(f32) + expert_sum).astype(bf16)
    return (layer_out, new_memory, new_max)
def solution(mesh):
    return jax.shard_map(
        body,
        mesh=mesh,
        in_specs=(
            P(("grp", "ep"), None),
            P(("grp", "ep"), None, None, None),
            P(("grp", "ep"), None),
            P(),
            P(None, "ep"),
            P(None, "ep"),
            P(None, "ep"),
            P(None, "ep"),
            P(),
            P(),
            P(),
            P(),
            P(None, "ep"),
            P(),
            P(("grp", "ep"), None),
            P(("grp", "ep"), None),
            P("ep", None, None),
            P("ep", None, None),
            P("ep", None, None),
        ),
        out_specs=(
            P(("grp", "ep"), None),
            P(("grp", "ep"), None, None, None),
            P(("grp", "ep"), None),
        ),
        check_vma=False,
    )
```

time: 162 us -> 156 us (0.963)
  waiting for transfers between devices: 59.5 us -> 38.1 us
  other arithmetic: 12.8 us -> 20.7 us
  blocking collectives: 15.5 us -> 22.9 us
  matrix products: 12.2 us -> 6.84 us
  local copies, waits for them, and re-layouts: 6.92 us -> 11.7 us
  Pallas kernels: 0 us -> 3.79 us
  starting transfers between devices: 53.2 us -> 50 us
    all_to_all x3, waiting for transfers between devices: 35.4 us -> 21.1 us  [exchange(): lax.all_to_all(blocks, 'ep', split_axis=0, concat_axis=0, tiled=True, axi...]
    mul x1 -> x3, other arithmetic: 0.01 us -> 8.17 us  [the longest x1 8.09 us: body(): decayed = carried[:, :, None, None] * memory_state]
    all_to_all x1, blocking collectives: 15.5 us -> 22.9 us  [exchange(): lax.all_to_all(blocks, 'ep', split_axis=0, concat_axis=0, tiled=True, axi...]
    ppermute x3 -> x8, starting transfers between devices: 17.6 us -> 11.4 us  [partner(): lax.ppermute(block, 'ep', [(i, i ^ 1) for i in range(lax.axis_size('ep'))])]
    all_to_all x1, waiting for transfers between devices: 22 us -> 15.8 us  [body(): lax.all_to_all(results, 'ep', split_axis=0, concat_axis=0, tiled=True)]
    dot_general x7 -> x2, matrix products: 7.87 us -> 1.79 us  [the longest x1 1.56 us: body(): lax.dot_general(same_mixed, tables[4], (((1,), (1,)), ((), ())), preferre...]
    pallas_call x0 -> x2, Pallas kernels: none -> 3.79 us  [the longest x1 2.77 us: body(): pl.pallas_call(project_kernel, out_shape=jax.ShapeDtypeStruct((half_rows,...]
    all_to_all x3, starting transfers between devices: 29.1 us -> 32.7 us  [exchange(): lax.all_to_all(blocks, 'ep', split_axis=0, concat_axis=0, tiled=True, axi...]
  transfers between devices with their start and end apart: 7 -> 12, of which waited for: 6 -> 4; matrix products, arithmetic and copies ran while one was open for 4% -> 16% of each run, Pallas kernels for 0% -> 0%
where the time goes in v2:
time: 156 us; the launch traced here: 155 us
  starting transfers between devices  50 us (32%)
  waiting for transfers between devices  38.1 us (24%)
  blocking collectives  22.9 us (15%)
  other arithmetic  20.7 us (13%)
  local copies, waits for them, and re-layouts  11.7 us (8%)
  matrix products  6.84 us (4%)
  Pallas kernels  3.79 us (2%)
    all_to_all x3, starting transfers between devices, exchange(): lax.all_to_all(blocks, 'ep', split_axis=0, concat_axis=0, tiled=True, axi...  32.7 us
    all_to_all x1, blocking collectives, exchange(): lax.all_to_all(blocks, 'ep', split_axis=0, concat_axis=0, tiled=True, axi...  22.9 us
    all_to_all x3, waiting for transfers between devices, exchange(): lax.all_to_all(blocks, 'ep', split_axis=0, concat_axis=0, tiled=True, axi...  21.1 us
    all_to_all x1, waiting for transfers between devices, body(): lax.all_to_all(results, 'ep', split_axis=0, concat_axis=0, tiled=True)  15.8 us
    ppermute x8, starting transfers between devices, partner(): lax.ppermute(block, 'ep', [(i, i ^ 1) for i in range(lax.axis_size('ep'))])  11.4 us
    mul x1, other arithmetic, body(): decayed = carried[:, :, None, None] * memory_state  8.09 us
    add x1, other arithmetic, body(): decayed + (written[:, :, None] * key_heads)[:, :, :, None] * value_heads[...  6.02 us
    all_to_all x1, starting transfers between devices, body(): lax.all_to_all(results, 'ep', split_axis=0, concat_axis=0, tiled=True)  5.94 us
  transfers between devices with their start and end apart: 12, of which 4 were waited for; matrix products, arithmetic and copies ran while one was open for 16% of the time, Pallas kernels for 0%

profile of v2, /device:TPU:69, one launch (start us, length us, event | category | flops | bytes accessed | tf_op | source)
XLA Modules:
  0.0 155.2 jit_solution(754503993220292217)
XLA Ops:
  0.6 1.7 %broadcast_in_dim.27 = bf16[16,4,2048]{2,1,0:T(4,128)(2,1)} broadcast(bf16[4,2048]{1,0:T(4,128)(2,1)} %param.19), dimensions={1,2} | broadcast | bytes 278528 | tf_op jit(solution)/shard_map/broadcast_in_dim | solution.py:32
  2.3 17.6 %all-to-all-start = ((bf16[16,4,2048]{2,1,0:T(4,128)(2,1)}), bf16[16,4,2048]{2,1,0:T(4,128)(2,1)S(1)}, u32[]{:S(2)}, u32[]{:S(2)}) async-start(bf16[16,4,2048]{2,1,0:T(4,128)(2,1)} %broadcast_in_dim.27), calls=%async_computation | async-start | bytes 524288 | tf_op jit(solution)/shard_map/all_to_all | solution.py:20
  19.9 1.0 collective-permute-start.3
  20.9 0.1 collective-permute-start.2
  21.0 0.4 collective-permute-start.1
  21.4 0.1 collective-permute-start
  21.6 0.8 fusion.40
  22.4 0.8 fusion.42
  23.2 0.9 fusion.44
  24.1 0.9 exponential_multiply_fusion
  25.2 0.8 convert_reduce_fusion.1
  26.0 0.9 select_reduce_fusion
  26.9 8.1 %broadcast_multiply_fusion.refs_0_ = f32[4,4,256,512]{3,2,1,0:T(8,128)} fusion(f32[4,4,256,512]{3,2,1,0:T(8,128)} %param.20, f32[4,4]{1,0:T(4,128)S(1)} %subtract_exponential_fusion), kind=kLoop, calls=%fused_computation.2 | loop fusion | flops 2097152 | bytes 16777280 | tf_op jit(solution)/shard_map/mul | solution.py:140
  35.2 0.1 maximum_select_fusion.1
  35.4 0.6 copy-done.5
  36.0 0.1 maximum_select_fusion
  36.1 1.3 pad_maximum_fusion.table
  37.4 0.8 reshape.194.rows
  38.2 2.8 %project.1 = bf16[64,384]{1,0:T(8,128)(2,1)} custom-call(bf16[64,2048]{1,0:T(8,128)(2,1)} %reshape.194.rows, f32[1,2048]{1,0:T(1,128)} %bitcast.62, bf16[384,2048]{1,0:T(8,128)(2,1)} %pad_maximum_fusion.table), custom_call_target="tpu_custom_call" | custom-call | tf_op jit(solution)/shard_map/project/pallas_call | solution.py:151
  41.0 0.8 reshape.196
  41.9 22.9 %all_to_all.25 = bf16[16,4,512]{2,1,0:T(4,128)(2,1)S(1)} all-to-all(bf16[16,4,512]{2,1,0:T(4,128)(2,1)S(1)} %pad_maximum_fusion.1), channel_id=1, replica_groups={{0,2,4,6,8,10,12,14,16,18,20,22,24,26,28,30},{1,3,5,7,9,11,13,15,17,19,..., dimensions={0} | all-to-all | bytes 131072 | tf_op jit(solution)/shard_map/all_to_all | solution.py:20
  64.8 3.4 %copy-done.1 = f32[4,4,256,512]{3,2,1,0:T(8,128)S(1)} copy-done((f32[4,4,256,512]{3,2,1,0:T(8,128)S(1)}, f32[4,4,256,512]{3,2,1,0:T(8,128)}, u32[]{:S(2)}) %copy-start.1) | copy-done | bytes 8388632
  68.2 1.0 readout.1
  69.2 0.8 broadcast_in_dim.38
  70.0 4.1 %all-to-all-start.2 = ((bf16[16,4,2048]{2,1,0:T(4,128)(2,1)}), bf16[16,4,2048]{2,1,0:T(4,128)(2,1)S(1)}, u32[]{:S(2)}, u32[]{:S(2)}) async-start(bf16[16,4,2048]{2,1,0:T(4,128)(2,1)} %broadcast_in_dim.38), calls=%async_computation.2 | async-start | bytes 524288 | tf_op jit(solution)/shard_map/all_to_all | solution.py:20
  74.1 2.1 %collective-permute-start.6 = (bf16[64,2048]{1,0:T(8,128)(2,1)}, bf16[64,2048]{1,0:T(8,128)(2,1)}, u32[]{:S(2)}, u32[]{:S(2)}) collective-permute-start(bf16[64,2048]{1,0:T(8,128)(2,1)} %bitcast.13), channel_id=1, source_target_pairs={{0,1},{1,0},{2,3},{3,2},{4,5},{5,4},{6,7},{7,6},{8,9},{9,8},{10,11... | collective-permute-start | bytes 786440 | tf_op jit(solution)/shard_map/ppermute | solution.py:36
  76.6 0.5 collective-permute-start.4
  77.0 9.6 %all-to-all-done.2 = bf16[16,4,2048]{2,1,0:T(4,128)(2,1)S(1)} async-done(((bf16[16,4,2048]{2,1,0:T(4,128)(2,1)}), bf16[16,4,2048]{2,1,0:T(4,128)(2,1)S(1)}, u32[]{:S(2)}, u32[]{:S(2)}) %all-to-all-start.2) | async-done | bytes 262176 | tf_op jit(solution)/shard_map/all_to_all | solution.py:20
  86.7 1.6 %convolution_convert_fusion.1 = bf16[64,128]{1,0:T(8,128)(2,1)S(1)} fusion(bf16[64,2048]{1,0:T(8,128)(2,1)S(1)} %reshape.199, bf16[64,2048]{1,0:T(8,128)(2,1)} %collective-permute-done.6, bf16[64,2048]{1,0:T(8,128)(2,1)} %bitcast.13, pred[]{:T(512)S(6)} %eq.28), kind=kOutput, calls=%fused_computation.14 | convolution fusion | flops 35921920 | bytes 802817 | tf_op jit(solution)/shard_map/dot_general | solution.py:198
  88.3 0.7 broadcast_in_dim.39
  89.0 11.1 %all-to-all-start.3 = ((bf16[16,64,128]{2,1,0:T(8,128)(2,1)}), bf16[16,64,128]{2,1,0:T(8,128)(2,1)S(1)}, u32[]{:S(2)}, u32[]{:S(2)}) async-start(bf16[16,64,128]{2,1,0:T(8,128)(2,1)} %broadcast_in_dim.39), calls=%async_computation.3 | async-start | bytes 524288 | tf_op jit(solution)/shard_map/all_to_all | solution.py:20
  100.2 0.1 compare_reduce_fusion.1
  100.5 0.1 compare_reduce_fusion
  101.0 0.1 select_n.67
  101.1 11.5 %all-to-all-done.3 = bf16[16,64,128]{2,1,0:T(8,128)(2,1)S(1)} async-done(((bf16[16,64,128]{2,1,0:T(8,128)(2,1)}), bf16[16,64,128]{2,1,0:T(8,128)(2,1)S(1)}, u32[]{:S(2)}, u32[]{:S(2)}) %all-to-all-start.3) | async-done | bytes 262176 | tf_op jit(solution)/shard_map/all_to_all | solution.py:20
  112.6 7.1 %collective-permute-start.7 = (bf16[16,64,128]{2,1,0:T(8,128)(2,1)S(1)}, bf16[16,64,128]{2,1,0:T(8,128)(2,1)S(1)}, u32[]{:S(2)}, u32[]{:S(2)}) collective-permute-start(bf16[16,64,128]{2,1,0:T(8,128)(2,1)S(1)} %all-to-all-done.3), channel_id=1, source_target_pairs={{0,1},{1,0},{2,3},{3,2},{4,5},{5,4},{6,7},{7,6},{8,9},{9,8},{10,11... | collective-permute-start | bytes 786440 | tf_op jit(solution)/shard_map/ppermute | solution.py:36
  119.8 1.1 collective-permute-done.7
  120.9 0.2 fusion.26
  121.2 0.2 fusion
  121.4 0.2 fusion.15
  121.6 0.5 fusion.4
  122.2 2.6 %convolution_convert_fusion = bf16[64,2048]{1,0:T(8,128)(2,1)S(1)} fusion(bf16[1,512,2048]{2,1,0:T(8,128)(2,1)S(1)} %copy-done, bf16[1,2048,512]{2,1,0:T(8,128)(2,1)} %param.36, f32[64,512]{1,0:T(8,128)S(1)} %fusion.4, f32[2048]{0:T(1024)S(1)} %copy-done.8, f32[64]{0:T(128)S(1)} %add_rsqrt_fusion, bf16[68,2048]{1,0:T(8,128)(2,1)S(1)} %fusion), kind=kOutput, calls=%fused_computation.5 | convolution fusion | flops 269287424 | bytes 4858368 | tf_op jit(solution)/shard_map/dot_general | solution.py:231
  124.7 0.9 reshape.202
  125.6 5.9 %all-to-all-start.4 = ((bf16[32,2,2048]{2,1,0:T(2,128)(2,1)}), bf16[32,2,2048]{2,1,0:T(2,128)(2,1)S(1)}, u32[]{:S(2)}, u32[]{:S(2)}) async-start(bf16[32,2,2048]{2,1,0:T(2,128)(2,1)} %reshape.202), calls=%async_computation.4 | async-start | bytes 524288 | tf_op jit(solution)/shard_map/all_to_all | solution.py:235
  131.8 6.0 %multiply_add_fusion = f32[4,4,256,512]{3,2,1,0:T(8,128)} fusion(f32[4,4,256,512]{3,2,1,0:T(8,128)} %broadcast_multiply_fusion.refs_0_, f32[4,4,512]{2,1,0:T(4,128)S(1)} %reshape.205, f32[4,4,256]{2,1,0:T(4,128)S(1)} %broadcast_multiply_fusion.1), kind=kLoop, calls=%fused_computation.1 | loop fusion | flops 4194304 | bytes 16826368 | tf_op jit(solution)/shard_map/add | solution.py:195
  137.8 15.8 %all-to-all-done.4 = bf16[32,2,2048]{2,1,0:T(2,128)(2,1)S(1)} async-done(((bf16[32,2,2048]{2,1,0:T(2,128)(2,1)}), bf16[32,2,2048]{2,1,0:T(2,128)(2,1)S(1)}, u32[]{:S(2)}, u32[]{:S(2)}) %all-to-all-start.4) | async-done | bytes 262176 | tf_op jit(solution)/shard_map/all_to_all | solution.py:235
  153.8 0.6 gather_fusion
  154.6 0.6 add_convert_fusion
  (81 shorter events, 2.2 us)
Async XLA Ops:
  0.6 121.5 %copy-start = (bf16[1,512,2048]{2,1,0:T(8,128)(2,1)S(1)}, bf16[1,512,2048]{2,1,0:T(8,128)(2,1)}, u32[]{:S(2)}) copy-start(bf16[1,512,2048]{2,1,0:T(8,128)(2,1)} %param.37) | copy-start | bytes 6291460
  2.3 35.1 %all-to-all-start = ((bf16[16,4,2048]{2,1,0:T(4,128)(2,1)}), bf16[16,4,2048]{2,1,0:T(4,128)(2,1)S(1)}, u32[]{:S(2)}, u32[]{:S(2)}) async-start(bf16[16,4,2048]{2,1,0:T(4,128)(2,1)} %broadcast_in_dim.27), calls=%async_computation | async-start | bytes 524288 | tf_op jit(solution)/shard_map/all_to_all | solution.py:20
  19.9 15.3 %collective-permute-start.3 = (bf16[64,2048]{1,0:T(8,128)(2,1)}, bf16[64,2048]{1,0:T(8,128)(2,1)S(1)}, u32[]{:S(2)}, u32[]{:S(2)}) collective-permute-start(bf16[64,2048]{1,0:T(8,128)(2,1)} %bitcast.54), channel_id=1, source_target_pairs={{0,1},{1,0},{2,3},{3,2},{4,5},{5,4},{6,7},{7,6},{8,9},{9,8},{10,11... | collective-permute-start | bytes 786440 | tf_op jit(solution)/shard_map/ppermute | solution.py:36
  20.9 14.4 %collective-permute-start.2 = (bf16[64,2048]{1,0:T(8,128)(2,1)}, bf16[64,2048]{1,0:T(8,128)(2,1)S(1)}, u32[]{:S(2)}, u32[]{:S(2)}) collective-permute-start(bf16[64,2048]{1,0:T(8,128)(2,1)} %bitcast.56), channel_id=1, source_target_pairs={{0,1},{1,0},{2,3},{3,2},{4,5},{5,4},{6,7},{7,6},{8,9},{9,8},{10,11... | collective-permute-start | bytes 786440 | tf_op jit(solution)/shard_map/ppermute | solution.py:36
  21.0 14.0 %collective-permute-start.1 = (bf16[32,2048]{1,0:T(8,128)(2,1)}, bf16[32,2048]{1,0:T(8,128)(2,1)S(1)}, u32[]{:S(2)}, u32[]{:S(2)}) collective-permute-start(bf16[32,2048]{1,0:T(8,128)(2,1)} %bitcast.58), channel_id=1, source_target_pairs={{0,1},{1,0},{2,3},{3,2},{4,5},{5,4},{6,7},{7,6},{8,9},{9,8},{10,11... | collective-permute-start | bytes 393224 | tf_op jit(solution)/shard_map/ppermute | solution.py:36
  21.4 13.7 %collective-permute-start = (bf16[32,2048]{1,0:T(8,128)(2,1)}, bf16[32,2048]{1,0:T(8,128)(2,1)S(1)}, u32[]{:S(2)}, u32[]{:S(2)}) collective-permute-start(bf16[32,2048]{1,0:T(8,128)(2,1)} %bitcast.60), channel_id=1, source_target_pairs={{0,1},{1,0},{2,3},{3,2},{4,5},{5,4},{6,7},{7,6},{8,9},{9,8},{10,11... | collective-permute-start | bytes 393224 | tf_op jit(solution)/shard_map/ppermute | solution.py:36
  25.0 10.1 %copy-start.12 = (f32[4,4]{1,0:T(4,128)}, f32[4,4]{1,0:T(4,128)S(1)}, u32[]{:S(2)}) copy-start(f32[4,4]{1,0:T(4,128)S(1)} %get-tuple-element.14) | copy-start | bytes 196
  26.9 8.1 %copy-start.9 = (s32[4,4]{1,0:T(4,128)S(1)}, s32[4,4]{1,0:T(4,128)}, u32[]{:S(2)}) copy-start(s32[4,4]{1,0:T(4,128)} %param.33) | copy-start | bytes 196
  26.9 8.2 %copy-start.6 = (bf16[2048,32]{0,1:T(8,128)(2,1)S(1)}, bf16[2048,32]{0,1:T(8,128)(2,1)}, u32[]{:S(2)}) copy-start(bf16[2048,32]{0,1:T(8,128)(2,1)} %param.24) | copy-start | bytes 393220
  26.9 8.2 %copy-start.7 = (bf16[2048,32]{0,1:T(8,128)(2,1)S(1)}, bf16[2048,32]{0,1:T(8,128)(2,1)}, u32[]{:S(2)}) copy-start(bf16[2048,32]{0,1:T(8,128)(2,1)} %param.23) | copy-start | bytes 393220
  26.9 8.3 %copy-start.4 = (bf16[2048,64]{0,1:T(8,128)(2,1)S(1)}, bf16[2048,64]{0,1:T(8,128)(2,1)}, u32[]{:S(2)}) copy-start(bf16[2048,64]{0,1:T(8,128)(2,1)} %param.26) | copy-start | bytes 786436
  35.0 1.0 copy-start.5
  36.1 2.1 %copy-start.10 = (f32[2048]{0:T(1024)S(1)}, f32[2048]{0:T(1024)}, u32[]{:S(2)}) copy-start(f32[2048]{0:T(1024)} %param.30) | copy-start | bytes 24580
  64.8 3.4 %copy-start.1 = (f32[4,4,256,512]{3,2,1,0:T(8,128)S(1)}, f32[4,4,256,512]{3,2,1,0:T(8,128)}, u32[]{:S(2)}) copy-start(f32[4,4,256,512]{3,2,1,0:T(8,128)} %broadcast_multiply_fusion.refs_0_) | copy-start | bytes 25165828
  68.2 8.3 %copy-start.2 = (bf16[64,2048]{1,0:T(8,128)(2,1)S(1)}, bf16[64,2048]{1,0:T(8,128)(2,1)}, u32[]{:S(2)}) copy-start(bf16[64,2048]{1,0:T(8,128)(2,1)} %reshape.194.rows) | copy-start | bytes 786436
  70.0 16.6 %all-to-all-start.2 = ((bf16[16,4,2048]{2,1,0:T(4,128)(2,1)}), bf16[16,4,2048]{2,1,0:T(4,128)(2,1)S(1)}, u32[]{:S(2)}, u32[]{:S(2)}) async-start(bf16[16,4,2048]{2,1,0:T(4,128)(2,1)} %broadcast_in_dim.38), calls=%async_computation.2 | async-start | bytes 524288 | tf_op jit(solution)/shard_map/all_to_all | solution.py:20
  74.1 12.6 %collective-permute-start.6 = (bf16[64,2048]{1,0:T(8,128)(2,1)}, bf16[64,2048]{1,0:T(8,128)(2,1)}, u32[]{:S(2)}, u32[]{:S(2)}) collective-permute-start(bf16[64,2048]{1,0:T(8,128)(2,1)} %bitcast.13), channel_id=1, source_target_pairs={{0,1},{1,0},{2,3},{3,2},{4,5},{5,4},{6,7},{7,6},{8,9},{9,8},{10,11... | collective-permute-start | bytes 786440 | tf_op jit(solution)/shard_map/ppermute | solution.py:36
  76.5 44.7 %collective-permute-start.5 = (bf16[64,2048]{1,0:T(8,128)(2,1)S(1)}, bf16[64,2048]{1,0:T(8,128)(2,1)S(1)}, u32[]{:S(2)}, u32[]{:S(2)}) collective-permute-start(bf16[64,2048]{1,0:T(8,128)(2,1)S(1)} %copy-done.2), channel_id=1, source_target_pairs={{0,1},{1,0},{2,3},{3,2},{4,5},{5,4},{6,7},{7,6},{8,9},{9,8},{10,11... | collective-permute-start | bytes 786440 | tf_op jit(solution)/shard_map/ppermute | solution.py:36
  76.6 23.9 %collective-permute-start.4 = (bf16[64,128]{1,0:T(8,128)(2,1)S(1)}, bf16[64,128]{1,0:T(8,128)(2,1)S(1)}, u32[]{:S(2)}, u32[]{:S(2)}) collective-permute-start(bf16[64,128]{1,0:T(8,128)(2,1)S(1)} %slice.31), channel_id=1, source_target_pairs={{0,1},{1,0},{2,3},{3,2},{4,5},{5,4},{6,7},{7,6},{8,9},{9,8},{10,11... | collective-permute-start | bytes 49160 | tf_op jit(solution)/shard_map/ppermute | solution.py:36
  89.0 23.6 %all-to-all-start.3 = ((bf16[16,64,128]{2,1,0:T(8,128)(2,1)}), bf16[16,64,128]{2,1,0:T(8,128)(2,1)S(1)}, u32[]{:S(2)}, u32[]{:S(2)}) async-start(bf16[16,64,128]{2,1,0:T(8,128)(2,1)} %broadcast_in_dim.39), calls=%async_computation.3 | async-start | bytes 524288 | tf_op jit(solution)/shard_map/all_to_all | solution.py:20
  100.1 21.5 %copy-start.8 = (f32[2048]{0:T(1024)S(1)}, f32[2048]{0:T(1024)}, u32[]{:S(2)}) copy-start(f32[2048]{0:T(1024)} %param.32) | copy-start | bytes 24580
  112.6 9.0 %copy-start.3 = (bf16[1,2048,512]{2,1,0:T(8,128)(2,1)S(1)}, bf16[1,2048,512]{2,1,0:T(8,128)(2,1)}, u32[]{:S(2)}) copy-start(bf16[1,2048,512]{2,1,0:T(8,128)(2,1)} %param.35) | copy-start | bytes 6291460
  112.6 8.3 %collective-permute-start.7 = (bf16[16,64,128]{2,1,0:T(8,128)(2,1)S(1)}, bf16[16,64,128]{2,1,0:T(8,128)(2,1)S(1)}, u32[]{:S(2)}, u32[]{:S(2)}) collective-permute-start(bf16[16,64,128]{2,1,0:T(8,128)(2,1)S(1)} %all-to-all-done.3), channel_id=1, source_target_pairs={{0,1},{1,0},{2,3},{3,2},{4,5},{5,4},{6,7},{7,6},{8,9},{9,8},{10,11... | collective-permute-start | bytes 786440 | tf_op jit(solution)/shard_map/ppermute | solution.py:36
  125.6 28.1 %all-to-all-start.4 = ((bf16[32,2,2048]{2,1,0:T(2,128)(2,1)}), bf16[32,2,2048]{2,1,0:T(2,128)(2,1)S(1)}, u32[]{:S(2)}, u32[]{:S(2)}) async-start(bf16[32,2,2048]{2,1,0:T(2,128)(2,1)} %reshape.202), calls=%async_computation.4 | async-start | bytes 524288 | tf_op jit(solution)/shard_map/all_to_all | solution.py:235
  131.8 22.6 %copy-start.11 = (f32[4,4]{1,0:T(4,128)S(1)}, f32[4,4]{1,0:T(4,128)}, u32[]{:S(2)}) copy-start(f32[4,4]{1,0:T(4,128)} %param.34) | copy-start | bytes 196

commit v3 on v2

--- a/solution.py
+++ b/solution.py
@@ -36,27 +36,96 @@
     return lax.ppermute(block, "ep", [(i, i ^ 1) for i in range(lax.axis_size("ep"))])
 
 
-def project_kernel(rows, gain, table, out):
-    entries = rows[...].astype(f32)
-    normed = scaled_norm(entries, gain[...]).astype(bf16)
-    out[...] = lax.dot_general(
+def gate_kernel(key_size, tokens, gain, in_table, forget_table, bias, last_max, head_gain, new_max, carried, written, carried_rows, weight_rows, gain_rows):
+    seqs = tokens.shape[0]
+    heads, chips = bias.shape[1], head_gain.shape[0]
+    normed = scaled_norm(tokens[...].astype(f32), gain[...]).astype(bf16)
+
+    def logits(table):
+        return lax.dot_general(
+            normed, table[...], (((1,), (1,)), ((), ())), preferred_element_type=f32
+        )
+
+    input_logit = logits(in_table)
+    forget_logit = logits(forget_table) + bias[...]
+    log_forget = jnp.minimum(forget_logit, 0.0) - jnp.log1p(jnp.exp(-jnp.abs(forget_logit)))
+    shifted = log_forget + last_max[...]
+    top = jnp.maximum(shifted, input_logit)
+    weight = jnp.exp(input_logit - top) * key_size ** (-0.5)
+    kept = jnp.exp(shifted - top)
+    new_max[...] = top
+    carried[...] = kept
+    written[...] = weight
+    for chip in range(chips):
+        head = chip // (chips // heads)
+        rows = pl.ds(chip * seqs, seqs)
+        carried_rows[rows, :] = jnp.broadcast_to(kept[:, head : head + 1], (seqs, lanes))
+        weight_rows[rows, :] = jnp.broadcast_to(weight[:, head : head + 1], (seqs, lanes))
+        gain_rows[rows, :] = jnp.broadcast_to(head_gain[chip : chip + 1, :], (seqs, lanes))
+
+
+def gather_tables(core, tables, out):
+    start = 0
+    for mine, theirs in zip(tables[::2], tables[1::2]):
+        count = mine.shape[0]
+        own = pl.multiple_of(start + core[0] * count, count)
+        other = pl.multiple_of(start + (1 - core[0]) * count, count)
+        out[pl.ds(own, count), :] = mine[...]
+        out[pl.ds(other, count), :] = theirs[...]
+        start += 2 * count
+
+
+def project_kernel(core, blocks, gain, routing, *refs):
+    tables, (out, table, rows) = refs[:-3], refs[-3:]
+    chips, seqs = blocks.shape[:2]
+    gather_tables(core, tables, table)
+    for chip in range(chips):
+        rows[chip * seqs : (chip + 1) * seqs, :] = blocks[chip].astype(f32)
+    normed = scaled_norm(rows[...], gain[...]).astype(bf16)
+    columns = lax.dot_general(
         normed, table[...], (((1,), (1,)), ((), ())), preferred_element_type=f32
+    )
+    total = columns.shape[1]
+    for chip in range(chips):
+        out[chip, :, :total] = columns[chip * seqs : (chip + 1) * seqs, :].astype(bf16)
+        out[chip, :, total:] = routing[...]
+
+
+def mix_kernel(core, blocks, mine, theirs, out, table, rows):
+    chips, seqs = blocks.shape[:2]
+    gather_tables(core, (mine, theirs), table)
+    for chip in range(chips):
+        rows[chip * seqs : (chip + 1) * seqs, :] = blocks[chip].astype(f32)
+    columns = lax.dot_general(
+        rows[...].astype(bf16), table[...], (((1,), (1,)), ((), ())), preferred_element_type=f32
     ).astype(bf16)
-
-
-def readout_kernel(chips, decayed, received, weight, gain, out, sums):
-    seqs, heads, keys, values = decayed.shape
+    for chip in range(chips):
+        out[chip] = columns
+
+
+def readout_kernel(state, received, carried, weight, gain, out, sums, flat, memory, arrived):
+    seqs, heads, keys, values = state.shape
+    chips = received.shape[0]
     per_head = chips // heads
     part = keys // per_head
-    flat = received[...].astype(f32)
+    copies = {}
+    for head in range(heads):
+        for seq in range(seqs):
+            copies[head, seq] = pltpu.make_async_copy(
+                state.at[seq, head], memory.at[seq, head], arrived.at[seq, head]
+            )
+            copies[head, seq].start()
+    for chip in range(chips):
+        flat[chip * seqs : (chip + 1) * seqs, :] = received[chip].astype(f32)
     pairs = flat[:, :lanes]
     columns = pairs.T
     for head in range(heads):
         for seq in range(seqs):
+            copies[head, seq].wait()
             total = jnp.zeros((8, values), f32)
             for j in range(per_head):
                 at = (head * per_head + j) * seqs + seq
-                block = decayed[seq, head, j * part : (j + 1) * part, :]
+                block = memory[seq, head, j * part : (j + 1) * part, :]
                 terms = block * columns[:part, at : at + 1]
                 total = total + jnp.sum(terms.reshape(part // 8, 8, values), axis=0)
             row = jnp.sum(total, axis=0, keepdims=True)
@@ -73,10 +142,14 @@
 
     products = pairs * jnp.concatenate([pairs[:, part:], pairs[:, :part]], axis=1)
     match = head_total(products) * 0.5
-    readout = sums[...] + (weight[...] * match) * flat[:, lanes : 2 * lanes]
+    readout = carried[...] * sums[...] + (weight[...] * match) * flat[:, lanes : 2 * lanes]
     scale = lax.rsqrt(head_total(readout * readout) / values + epsilon)
     gates = jax.nn.sigmoid(flat[:, 2 * lanes : 3 * lanes])
-    out[...] = (readout * scale * gain[...] * gates).astype(bf16)
+    mixed = readout * scale * gain[...] * gates
+    for chip in range(chips):
+        tile = mixed[chip * seqs : (chip + 1) * seqs, :].astype(bf16)
+        for copy in range(chips):
+            out[copy, :, chip * lanes : (chip + 1) * lanes] = tile
 
 
 def body(
@@ -112,73 +185,67 @@
     capacity = min(seq_rows, 2)
     choices = routed_experts.shape[1]
 
-    same_tokens = spread(tokens).reshape(half_rows, width)
-
-    tables = []
+    same_tokens = spread(tokens)
+
+    pairs = []
     for table in (query_weight, key_weight, value_weight, output_gate, output_weight):
-        mine = table.T
-        theirs = partner(mine)
-        tables.append(
-            jnp.where(
-                core == 0,
-                jnp.concatenate([mine, theirs], axis=0),
-                jnp.concatenate([theirs, mine], axis=0),
-            )
-        )
-    table = jnp.concatenate(tables[:4], axis=0)
-    total = table.shape[0]
-
-    inputs = tokens.astype(f32)
-    normed = scaled_norm(inputs, norm_gain).astype(bf16)
-    input_logit = jnp.dot(normed, input_gate, preferred_element_type=f32)
-    log_forget = jax.nn.log_sigmoid(
-        jnp.dot(normed, forget_gate, preferred_element_type=f32) + forget_bias
-    )
-    new_max = jnp.maximum(log_forget + max_state, input_logit)
-    carried = jnp.exp(log_forget + max_state - new_max)
-    written = jnp.exp(input_logit - new_max) * key_size ** (-0.5)
-    decayed = carried[:, :, None, None] * memory_state
+        pairs += [table.T, partner(table.T)]
+    total = sum(table.shape[0] for table in pairs[:-2])
+
     per_head = chips // head_count
-    by_chip = (head_count, per_head, seq_rows, lanes)
-    weight_rows = jnp.broadcast_to(written.T[:, None, :, None], by_chip).reshape(half_rows, lanes)
-    gain_rows = jnp.broadcast_to(
-        head_gain.reshape(head_count, per_head, 1, lanes), by_chip
-    ).reshape(half_rows, lanes)
-    same_tokens, table, decayed, weight_rows, gain_rows = lax.optimization_barrier(
-        (same_tokens, table, decayed, weight_rows, gain_rows)
-    )
-
-    projected = pl.pallas_call(
-        project_kernel,
-        out_shape=jax.ShapeDtypeStruct((half_rows, total), bf16),
-        in_specs=[whole] * 3,
-        out_specs=whole,
-        name="project",
-    )(same_tokens, norm_gain[None], table)
+    gate_shape = jax.ShapeDtypeStruct((seq_rows, head_count), f32)
+    row_shape = jax.ShapeDtypeStruct((half_rows, lanes), f32)
+    new_max, carried, written, carried_rows, weight_rows, gain_rows = pl.pallas_call(
+        lambda *refs: gate_kernel(key_size, *refs),
+        out_shape=(gate_shape,) * 3 + (row_shape,) * 3,
+        in_specs=[whole] * 7,
+        out_specs=(whole,) * 6,
+        compiler_params=pltpu.CompilerParams(vmem_limit_bytes=4 << 20),
+        name="gates",
+    )(
+        tokens,
+        norm_gain[None],
+        input_gate.T,
+        forget_gate.T,
+        forget_bias[None],
+        max_state,
+        head_gain.reshape(chips, lanes),
+    )
     routing = jnp.pad(routed_experts.astype(bf16), ((0, 0), (0, lanes - choices)))
+    same_tokens, pairs, carried_rows, weight_rows, gain_rows, routing = lax.optimization_barrier(
+        (same_tokens, pairs, carried_rows, weight_rows, gain_rows, routing)
+    )
+
+    scalar = pl.BlockSpec(memory_space=pltpu.SMEM)
     received = exchange(
-        jnp.concatenate(
-            [
-                projected.reshape(chips, seq_rows, total),
-                jnp.broadcast_to(routing[None], (chips, seq_rows, lanes)),
+        pl.pallas_call(
+            project_kernel,
+            out_shape=jax.ShapeDtypeStruct((chips, seq_rows, total + lanes), bf16),
+            in_specs=[scalar] + [whole] * (1 + len(pairs)),
+            out_specs=whole,
+            scratch_shapes=[pltpu.VMEM((total, width), bf16), pltpu.VMEM((half_rows, width), f32)],
+            compiler_params=pltpu.CompilerParams(vmem_limit_bytes=8 << 20),
+            name="project",
+        )(core[None], same_tokens, norm_gain[None], routing, *pairs[:-2])
+    )
+    same_mixed = exchange(
+        pl.pallas_call(
+            readout_kernel,
+            out_shape=jax.ShapeDtypeStruct((chips, seq_rows, width), bf16),
+            in_specs=[pl.BlockSpec(memory_space=pltpu.HBM)] + [whole] * 4,
+            out_specs=whole,
+            scratch_shapes=[
+                pltpu.VMEM((half_rows, lanes), f32),
+                pltpu.VMEM((half_rows, total + lanes), f32),
+                pltpu.VMEM(memory_state.shape, f32),
+                pltpu.SemaphoreType.DMA(memory_state.shape[:2]),
             ],
-            axis=2,
-        )
-    ).reshape(half_rows, total + lanes)
-
-    mixed = pl.pallas_call(
-        lambda *refs: readout_kernel(chips, *refs),
-        out_shape=jax.ShapeDtypeStruct((half_rows, lanes), bf16),
-        in_specs=[whole] * 4,
-        out_specs=whole,
-        scratch_shapes=[pltpu.VMEM((half_rows, lanes), f32)],
-        compiler_params=pltpu.CompilerParams(vmem_limit_bytes=24 << 20),
-        name="readout",
-    )(decayed, received, weight_rows, gain_rows)
-    mixed = mixed.reshape(chips, seq_rows, lanes).transpose(1, 0, 2).reshape(seq_rows, width)
-    same_mixed = spread(mixed).reshape(half_rows, width)
-
-    by_source = received.reshape(chips, seq_rows, total + lanes)
+            compiler_params=pltpu.CompilerParams(vmem_limit_bytes=48 << 20),
+            name="readout",
+        )(memory_state, received, carried_rows, weight_rows, gain_rows)
+    )
+
+    by_source = received
     edge = total // 6
 
     def own_columns(start, size):
@@ -192,18 +259,29 @@
     key_heads = own_columns(edge, edge)
     value_heads = own_columns(2 * edge, 2 * edge)
     new_memory = (
-        decayed + (written[:, :, None] * key_heads)[:, :, :, None] * value_heads[:, :, None, :]
-    )
-
-    columns = lax.dot_general(
-        same_mixed, tables[4], (((1,), (1,)), ((), ())), preferred_element_type=f32
-    ).astype(bf16)
-    same_branch = spread(columns)
+        carried[:, :, None, None] * memory_state
+        + (written[:, :, None] * key_heads)[:, :, :, None] * value_heads[:, :, None, :]
+    )
+
+    same_branch = exchange(
+        pl.pallas_call(
+            mix_kernel,
+            out_shape=jax.ShapeDtypeStruct((chips, half_rows, lanes), bf16),
+            in_specs=[scalar] + [whole] * 3,
+            out_specs=whole,
+            scratch_shapes=[pltpu.VMEM((lanes, width), bf16), pltpu.VMEM((half_rows, width), f32)],
+            compiler_params=pltpu.CompilerParams(vmem_limit_bytes=4 << 20),
+            name="mix",
+        )(core[None], same_mixed, *pairs[-2:])
+    )
     other_branch = partner(same_branch)
     other_tokens = partner(same_tokens)
 
-    same_routed = received[:, total : total + choices]
-    other_routed = partner(received[:, total:])[:, :choices]
+    same_tokens = same_tokens.reshape(half_rows, width)
+    other_tokens = other_tokens.reshape(half_rows, width)
+    same_routed = received[:, :, total:]
+    other_routed = partner(same_routed).reshape(half_rows, lanes)[:, :choices]
+    same_routed = same_routed.reshape(half_rows, lanes)[:, :choices]
     same_named = jnp.any(same_routed == me.astype(bf16), axis=1).astype(jnp.int32)
     other_named = jnp.any(other_routed == me.astype(bf16), axis=1).astype(jnp.int32)
     named = jnp.stack([same_named, other_named]).reshape(2, chips, seq_rows)
@@ -232,6 +310,7 @@
         .astype(bf16)
         .reshape(axis_size, capacity, width)
     )
+    routed_experts, results = lax.optimization_barrier((routed_experts, results))
     returned = lax.all_to_all(results, "ep", split_axis=0, concat_axis=0, tiled=True)
     expert_ids = jnp.arange(axis_size, dtype=jnp.int32)
     chosen = (routed_experts[:, :, None] == expert_ids[None, None, :]).astype(jnp.int32)

time: 156 us -> 151 us (0.968)
  blocking collectives: 22.9 us -> 0 us
  waiting for transfers between devices: 38.1 us -> 52.1 us
  other arithmetic: 20.7 us -> 9.59 us
  starting transfers between devices: 50 us -> 60.3 us
  Pallas kernels: 3.79 us -> 7.95 us
  local copies, waits for them, and re-layouts: 11.7 us -> 15.3 us
  matrix products: 6.84 us -> 3.54 us
    all_to_all x1 -> x0, blocking collectives: 22.9 us -> none  [exchange(): lax.all_to_all(blocks, 'ep', split_axis=0, concat_axis=0, tiled=True, axi...]
    all_to_all x3 -> x4, waiting for transfers between devices: 21.1 us -> 35.5 us  [exchange(): lax.all_to_all(blocks, 'ep', split_axis=0, concat_axis=0, tiled=True, axi...]
    all_to_all x3 -> x4, starting transfers between devices: 32.7 us -> 42.8 us  [exchange(): lax.all_to_all(blocks, 'ep', split_axis=0, concat_axis=0, tiled=True, axi...]
    mul x1 -> x0, other arithmetic: 8.09 us -> none  [body(): decayed = carried[:, :, None, None] * memory_state]
    unnamed x26 -> x40, local copies, waits for them, and re-layouts: 4.07 us -> 10.1 us
    pallas_call x2 -> x4, Pallas kernels: 3.79 us -> 7.95 us  [the longest x1 4.57 us: body(): pl.pallas_call(readout_kernel, out_shape=jax.ShapeDtypeStruct((chips, seq...]
    dot_general x3 -> x0, matrix products: 3.29 us -> none  [the longest x1 1.56 us: body(): lax.dot_general(same_mixed, tables[4], (((1,), (1,)), ((), ())), preferre...]
    broadcast_in_dim x3 -> x1, local copies, waits for them, and re-layouts: 3.21 us -> 1.67 us  [spread(): return exchange(jnp.broadcast_to(block[None], (chips,) + block.shape))]
  transfers between devices with their start and end apart: 12 -> 13, of which waited for: 4 -> 6; matrix products, arithmetic and copies ran while one was open for 16% -> 7% of each run, Pallas kernels for 0% -> 1%
where the time goes in v3:
time: 151 us; the launch traced here: 150 us
  starting transfers between devices  60.3 us (40%)
  waiting for transfers between devices  52.1 us (35%)
  local copies, waits for them, and re-layouts  15.3 us (10%)
  other arithmetic  9.59 us (6%)
  Pallas kernels  7.95 us (5%)
  matrix products  3.54 us (2%)
    all_to_all x4, starting transfers between devices, exchange(): lax.all_to_all(blocks, 'ep', split_axis=0, concat_axis=0, tiled=True, axi...  42.8 us
    all_to_all x4, waiting for transfers between devices, exchange(): lax.all_to_all(blocks, 'ep', split_axis=0, concat_axis=0, tiled=True, axi...  35.5 us
    all_to_all x1, waiting for transfers between devices, body(): lax.all_to_all(results, 'ep', split_axis=0, concat_axis=0, tiled=True)  15.5 us
    ppermute x8, starting transfers between devices, partner(): lax.ppermute(block, 'ep', [(i, i ^ 1) for i in range(lax.axis_size('ep'))])  11.4 us
    unnamed x40, local copies, waits for them, and re-layouts  10.1 us
    add x1, other arithmetic, body(): carried[:, :, None, None] * memory_state  6.17 us
    all_to_all x1, starting transfers between devices, body(): lax.all_to_all(results, 'ep', split_axis=0, concat_axis=0, tiled=True)  6.15 us
    pallas_call x1, Pallas kernels, body(): pl.pallas_call(readout_kernel, out_shape=jax.ShapeDtypeStruct((chips, seq...  4.57 us
  transfers between devices with their start and end apart: 13, of which 6 were waited for; matrix products, arithmetic and copies ran while one was open for 7% of the time, Pallas kernels for 1%

profile of v3, /device:TPU:69, one launch (start us, length us, event | category | flops | bytes accessed | tf_op | source)
XLA Modules:
  0.0 149.8 jit_solution(11070729205918446041)
XLA Ops:
  0.6 1.7 %broadcast_in_dim.14 = bf16[16,4,2048]{2,1,0:T(4,128)(2,1)} broadcast(bf16[4,2048]{1,0:T(4,128)(2,1)} %refs_0_.1), dimensions={1,2} | broadcast | bytes 278528 | tf_op jit(solution)/shard_map/broadcast_in_dim | solution.py:32
  2.3 17.6 %all-to-all-start = ((bf16[16,4,2048]{2,1,0:T(4,128)(2,1)}), bf16[16,4,2048]{2,1,0:T(4,128)(2,1)S(1)}, u32[]{:S(2)}, u32[]{:S(2)}) async-start(bf16[16,4,2048]{2,1,0:T(4,128)(2,1)} %broadcast_in_dim.14), calls=%async_computation | async-start | bytes 524288 | tf_op jit(solution)/shard_map/all_to_all | solution.py:20
  19.9 1.0 collective-permute-start.2
  20.9 0.1 collective-permute-start.3
  21.0 0.4 collective-permute-start.4
  21.6 0.4 collective-permute-start.1
  21.9 0.7 convert_element_type.93
  22.6 0.7 copy-done.6
  23.3 0.7 copy-done.9
  24.0 0.7 copy-done.11
  24.7 0.7 copy-done.12
  25.5 0.7 copy-done.13
  26.2 0.7 copy-done.14
  26.8 0.7 copy-done.15
  27.5 0.9 gates.1
  28.4 5.0 %all-to-all-done.blocks = bf16[16,4,2048]{2,1,0:T(4,128)(2,1)S(1)} async-done(((bf16[16,4,2048]{2,1,0:T(4,128)(2,1)}), bf16[16,4,2048]{2,1,0:T(4,128)(2,1)S(1)}, u32[]{:S(2)}, u32[]{:S(2)}) %all-to-all-start) | async-done | bytes 262176 | tf_op jit(solution)/shard_map/all_to_all | solution.py:20
  33.5 0.9 copy-done.1
  34.4 0.9 copy-done.2
  35.4 0.9 copy-done.4
  36.3 0.9 copy-done.5
  37.2 0.7 copy-done.10
  37.9 1.4 project.1
  39.3 10.5 %all-to-all-start.1 = ((bf16[16,4,512]{2,1,0:T(4,128)(2,1)}), bf16[16,4,512]{2,1,0:T(4,128)(2,1)S(1)}, u32[]{:S(2)}, u32[]{:S(2)}) async-start(bf16[16,4,512]{2,1,0:T(4,128)(2,1)} %project.1), calls=%async_computation.1 | async-start | bytes 131072 | tf_op jit(solution)/shard_map/all_to_all | solution.py:20
  50.0 11.2 %all-to-all-done.1.received = bf16[16,4,512]{2,1,0:T(4,128)(2,1)S(1)} async-done(((bf16[16,4,512]{2,1,0:T(4,128)(2,1)}), bf16[16,4,512]{2,1,0:T(4,128)(2,1)S(1)}, u32[]{:S(2)}, u32[]{:S(2)}) %all-to-all-start.1) | async-done | bytes 65568 | tf_op jit(solution)/shard_map/all_to_all | solution.py:20
  61.2 0.8 copy-done.8
  62.0 4.6 %readout.1 = bf16[16,4,2048]{2,1,0:T(4,128)(2,1)} custom-call(f32[4,4,256,512]{3,2,1,0:T(8,128)} %state.1, bf16[16,4,512]{2,1,0:T(4,128)(2,1)S(1)} %all-to-all-done.1.received, f32[64,128]{1,0:T(8,128)S(1)} %get-tuple-element.39.carried, f32[64,128]{1,0:T(8,128)S(1)} %get-tuple-element.40.weight, f32[64,128]{1,0:T(8,128)S(1)} %copy-done.8), custom_call_target="tpu_custom_call" | custom-call | tf_op jit(solution)/shard_map/readout/pallas_call | solution.py:232
  66.6 4.0 %all-to-all-start.2 = ((bf16[16,4,2048]{2,1,0:T(4,128)(2,1)}), bf16[16,4,2048]{2,1,0:T(4,128)(2,1)S(1)}, u32[]{:S(2)}, u32[]{:S(2)}) async-start(bf16[16,4,2048]{2,1,0:T(4,128)(2,1)} %readout.1), calls=%async_computation.2 | async-start | bytes 524288 | tf_op jit(solution)/shard_map/all_to_all | solution.py:20
  70.8 2.3 %collective-permute-start.6 = (bf16[16,4,2048]{2,1,0:T(4,128)(2,1)S(1)}, bf16[16,4,2048]{2,1,0:T(4,128)(2,1)}, u32[]{:S(2)}, u32[]{:S(2)}) collective-permute-start(bf16[16,4,2048]{2,1,0:T(4,128)(2,1)S(1)} %all-to-all-done.blocks), channel_id=1, source_target_pairs={{0,1},{1,0},{2,3},{3,2},{4,5},{5,4},{6,7},{7,6},{8,9},{9,8},{10,11... | collective-permute-start | bytes 786440 | tf_op jit(solution)/shard_map/ppermute | solution.py:36
  73.4 9.5 %all-to-all-done.2.blocks = bf16[16,4,2048]{2,1,0:T(4,128)(2,1)S(1)} async-done(((bf16[16,4,2048]{2,1,0:T(4,128)(2,1)}), bf16[16,4,2048]{2,1,0:T(4,128)(2,1)S(1)}, u32[]{:S(2)}, u32[]{:S(2)}) %all-to-all-start.2) | async-done | bytes 262176 | tf_op jit(solution)/shard_map/all_to_all | solution.py:20
  82.9 1.1 mix.1
  84.0 10.7 %all-to-all-start.3 = ((bf16[16,64,128]{2,1,0:T(8,128)(2,1)}), bf16[16,64,128]{2,1,0:T(8,128)(2,1)S(1)}, u32[]{:S(2)}, u32[]{:S(2)}) async-start(bf16[16,64,128]{2,1,0:T(8,128)(2,1)} %mix.1), calls=%async_computation.3 | async-start | bytes 524288 | tf_op jit(solution)/shard_map/all_to_all | solution.py:20
  95.1 0.8 compare_reduce_fusion
  96.4 1.0 reshape.177
  97.4 9.7 %all-to-all-done.3 = bf16[16,64,128]{2,1,0:T(8,128)(2,1)S(1)} async-done(((bf16[16,64,128]{2,1,0:T(8,128)(2,1)}), bf16[16,64,128]{2,1,0:T(8,128)(2,1)S(1)}, u32[]{:S(2)}, u32[]{:S(2)}) %all-to-all-start.3) | async-done | bytes 262176 | tf_op jit(solution)/shard_map/all_to_all | solution.py:20
  107.2 6.9 %collective-permute-start.7 = (bf16[16,64,128]{2,1,0:T(8,128)(2,1)S(1)}, bf16[16,64,128]{2,1,0:T(8,128)(2,1)S(1)}, u32[]{:S(2)}, u32[]{:S(2)}) collective-permute-start(bf16[16,64,128]{2,1,0:T(8,128)(2,1)S(1)} %all-to-all-done.3), channel_id=1, source_target_pairs={{0,1},{1,0},{2,3},{3,2},{4,5},{5,4},{6,7},{7,6},{8,9},{9,8},{10,11... | collective-permute-start | bytes 786440 | tf_op jit(solution)/shard_map/ppermute | solution.py:36
  114.1 1.1 collective-permute-done.7
  115.3 0.2 fusion.20
  115.5 0.2 fusion
  115.8 0.2 fusion.14
  115.9 0.5 fusion.4
  116.5 2.6 %convolution_convert_fusion = bf16[64,2048]{1,0:T(8,128)(2,1)S(1)} fusion(bf16[1,512,2048]{2,1,0:T(8,128)(2,1)S(1)} %copy-done, bf16[1,2048,512]{2,1,0:T(8,128)(2,1)} %param.36, f32[64,512]{1,0:T(8,128)S(1)} %fusion.4, f32[2048]{0:T(1024)S(1)} %copy-done.17, f32[64]{0:T(128)S(1)} %add_rsqrt_fusion, bf16[68,2048]{1,0:T(8,128)(2,1)S(1)} %fusion), kind=kOutput, calls=%fused_computation.4 | convolution fusion | flops 269287424 | bytes 4858368 | tf_op jit(solution)/shard_map/dot_general | solution.py:309
  119.0 0.9 reshape.180
  119.9 6.2 %all-to-all-start.4 = ((bf16[32,2,2048]{2,1,0:T(2,128)(2,1)}), bf16[32,2,2048]{2,1,0:T(2,128)(2,1)S(1)}, u32[]{:S(2)}, u32[]{:S(2)}) async-start(bf16[32,2,2048]{2,1,0:T(2,128)(2,1)} %reshape.180), calls=%async_computation.4 | async-start | bytes 524288 | tf_op jit(solution)/shard_map/all_to_all | solution.py:314
  126.1 6.2 %multiply_add_fusion = f32[4,4,256,512]{3,2,1,0:T(8,128)} fusion(f32[4,4,256,512]{3,2,1,0:T(8,128)} %state.1, f32[4,4,512]{2,1,0:T(4,128)S(1)} %reshape.183, f32[4,4,256]{2,1,0:T(4,128)S(1)} %broadcast_multiply_fusion, f32[4,4]{1,0:T(4,128)S(1)} %get-tuple-element.46), kind=kLoop, calls=%fused_computation.1 | loop fusion | flops 6291456 | bytes 16826432 | tf_op jit(solution)/shard_map/add | solution.py:262
  132.4 0.2 select_reduce_fusion
  132.7 15.5 %all-to-all-done.4 = bf16[32,2,2048]{2,1,0:T(2,128)(2,1)S(1)} async-done(((bf16[32,2,2048]{2,1,0:T(2,128)(2,1)}), bf16[32,2,2048]{2,1,0:T(2,128)(2,1)S(1)}, u32[]{:S(2)}, u32[]{:S(2)}) %all-to-all-start.4) | async-done | bytes 262176 | tf_op jit(solution)/shard_map/all_to_all | solution.py:314
  148.3 0.6 gather_fusion
  149.1 0.6 add_convert_fusion
  (74 shorter events, 2.3 us)
Async XLA Ops:
  0.6 115.8 %copy-start = (bf16[1,512,2048]{2,1,0:T(8,128)(2,1)S(1)}, bf16[1,512,2048]{2,1,0:T(8,128)(2,1)}, u32[]{:S(2)}) copy-start(bf16[1,512,2048]{2,1,0:T(8,128)(2,1)} %param.37) | copy-start | bytes 6291460
  2.3 31.1 %all-to-all-start = ((bf16[16,4,2048]{2,1,0:T(4,128)(2,1)}), bf16[16,4,2048]{2,1,0:T(4,128)(2,1)S(1)}, u32[]{:S(2)}, u32[]{:S(2)}) async-start(bf16[16,4,2048]{2,1,0:T(4,128)(2,1)} %broadcast_in_dim.14), calls=%async_computation | async-start | bytes 524288 | tf_op jit(solution)/shard_map/all_to_all | solution.py:20
  19.9 8.5 %collective-permute-start.2 = (bf16[64,2048]{1,0:T(8,128)(2,1)}, bf16[64,2048]{1,0:T(8,128)(2,1)S(1)}, u32[]{:S(2)}, u32[]{:S(2)}) collective-permute-start(bf16[64,2048]{1,0:T(8,128)(2,1)} %bitcast.45), channel_id=1, source_target_pairs={{0,1},{1,0},{2,3},{3,2},{4,5},{5,4},{6,7},{7,6},{8,9},{9,8},{10,11... | collective-permute-start | bytes 786440 | tf_op jit(solution)/shard_map/ppermute | solution.py:36
  20.9 7.5 %collective-permute-start.3 = (bf16[64,2048]{1,0:T(8,128)(2,1)}, bf16[64,2048]{1,0:T(8,128)(2,1)S(1)}, u32[]{:S(2)}, u32[]{:S(2)}) collective-permute-start(bf16[64,2048]{1,0:T(8,128)(2,1)} %bitcast.47), channel_id=1, source_target_pairs={{0,1},{1,0},{2,3},{3,2},{4,5},{5,4},{6,7},{7,6},{8,9},{9,8},{10,11... | collective-permute-start | bytes 786440 | tf_op jit(solution)/shard_map/ppermute | solution.py:36
  21.0 7.4 %collective-permute-start.4 = (bf16[64,2048]{1,0:T(8,128)(2,1)}, bf16[64,2048]{1,0:T(8,128)(2,1)S(1)}, u32[]{:S(2)}, u32[]{:S(2)}) collective-permute-start(bf16[64,2048]{1,0:T(8,128)(2,1)} %bitcast.49), channel_id=1, source_target_pairs={{0,1},{1,0},{2,3},{3,2},{4,5},{5,4},{6,7},{7,6},{8,9},{9,8},{10,11... | collective-permute-start | bytes 786440 | tf_op jit(solution)/shard_map/ppermute | solution.py:36
  21.4 7.0 %collective-permute-start = (bf16[32,2048]{1,0:T(8,128)(2,1)}, bf16[32,2048]{1,0:T(8,128)(2,1)S(1)}, u32[]{:S(2)}, u32[]{:S(2)}) collective-permute-start(bf16[32,2048]{1,0:T(8,128)(2,1)} %bitcast.51), channel_id=1, source_target_pairs={{0,1},{1,0},{2,3},{3,2},{4,5},{5,4},{6,7},{7,6},{8,9},{9,8},{10,11... | collective-permute-start | bytes 393224 | tf_op jit(solution)/shard_map/ppermute | solution.py:36
  21.6 6.8 %collective-permute-start.1 = (bf16[32,2048]{1,0:T(8,128)(2,1)}, bf16[32,2048]{1,0:T(8,128)(2,1)S(1)}, u32[]{:S(2)}, u32[]{:S(2)}) collective-permute-start(bf16[32,2048]{1,0:T(8,128)(2,1)} %bitcast.53), channel_id=1, source_target_pairs={{0,1},{1,0},{2,3},{3,2},{4,5},{5,4},{6,7},{7,6},{8,9},{9,8},{10,11... | collective-permute-start | bytes 393224 | tf_op jit(solution)/shard_map/ppermute | solution.py:36
  22.6 0.7 copy-start.6
  23.3 0.7 copy-start.9
  24.0 0.7 copy-start.11
  24.7 0.7 copy-start.12
  25.5 0.7 copy-start.13
  26.2 0.7 copy-start.14
  26.8 0.7 copy-start.15
  28.4 21.5 %copy-start.7 = (f32[64,128]{1,0:T(8,128)}, f32[64,128]{1,0:T(8,128)S(1)}, u32[]{:S(2)}) copy-start(f32[64,128]{1,0:T(8,128)S(1)} %get-tuple-element.41.gain) | copy-start | bytes 98308
  33.5 1.0 copy-start.1
  34.4 0.9 copy-start.2
  35.4 0.9 copy-start.4
  36.3 0.9 copy-start.5
  37.2 0.7 copy-start.10
  39.3 21.9 %all-to-all-start.1 = ((bf16[16,4,512]{2,1,0:T(4,128)(2,1)}), bf16[16,4,512]{2,1,0:T(4,128)(2,1)S(1)}, u32[]{:S(2)}, u32[]{:S(2)}) async-start(bf16[16,4,512]{2,1,0:T(4,128)(2,1)} %project.1), calls=%async_computation.1 | async-start | bytes 131072 | tf_op jit(solution)/shard_map/all_to_all | solution.py:20
  50.0 32.9 %copy-start.3 = (bf16[2048,64]{0,1:T(8,128)(2,1)S(1)}, bf16[2048,64]{0,1:T(8,128)(2,1)}, u32[]{:S(2)}) copy-start(bf16[2048,64]{0,1:T(8,128)(2,1)} %param.31) | copy-start | bytes 786436
  61.2 0.8 copy-start.8
  66.6 16.3 %all-to-all-start.2 = ((bf16[16,4,2048]{2,1,0:T(4,128)(2,1)}), bf16[16,4,2048]{2,1,0:T(4,128)(2,1)S(1)}, u32[]{:S(2)}, u32[]{:S(2)}) async-start(bf16[16,4,2048]{2,1,0:T(4,128)(2,1)} %readout.1), calls=%async_computation.2 | async-start | bytes 524288 | tf_op jit(solution)/shard_map/all_to_all | solution.py:20
  70.8 25.6 %collective-permute-start.6 = (bf16[16,4,2048]{2,1,0:T(4,128)(2,1)S(1)}, bf16[16,4,2048]{2,1,0:T(4,128)(2,1)}, u32[]{:S(2)}, u32[]{:S(2)}) collective-permute-start(bf16[16,4,2048]{2,1,0:T(4,128)(2,1)S(1)} %all-to-all-done.blocks), channel_id=1, source_target_pairs={{0,1},{1,0},{2,3},{3,2},{4,5},{5,4},{6,7},{7,6},{8,9},{9,8},{10,11... | collective-permute-start | bytes 786440 | tf_op jit(solution)/shard_map/ppermute | solution.py:36
  73.3 21.8 %collective-permute-start.5 = (bf16[16,4,128]{2,1,0:T(4,128)(2,1)S(1)}, bf16[16,4,128]{2,1,0:T(4,128)(2,1)}, u32[]{:S(2)}, u32[]{:S(2)}) collective-permute-start(bf16[16,4,128]{2,1,0:T(4,128)(2,1)S(1)} %get-tuple-element.50), channel_id=1, source_target_pairs={{0,1},{1,0},{2,3},{3,2},{4,5},{5,4},{6,7},{7,6},{8,9},{9,8},{10,11... | collective-permute-start | bytes 49160 | tf_op jit(solution)/shard_map/ppermute | solution.py:36
  84.0 23.2 %all-to-all-start.3 = ((bf16[16,64,128]{2,1,0:T(8,128)(2,1)}), bf16[16,64,128]{2,1,0:T(8,128)(2,1)S(1)}, u32[]{:S(2)}, u32[]{:S(2)}) async-start(bf16[16,64,128]{2,1,0:T(8,128)(2,1)} %mix.1), calls=%async_computation.3 | async-start | bytes 524288 | tf_op jit(solution)/shard_map/all_to_all | solution.py:20
  96.4 19.5 %copy-start.17 = (f32[2048]{0:T(1024)S(1)}, f32[2048]{0:T(1024)}, u32[]{:S(2)}) copy-start(f32[2048]{0:T(1024)} %param.32) | copy-start | bytes 24580
  107.2 8.7 %copy-start.16 = (bf16[1,2048,512]{2,1,0:T(8,128)(2,1)S(1)}, bf16[1,2048,512]{2,1,0:T(8,128)(2,1)}, u32[]{:S(2)}) copy-start(bf16[1,2048,512]{2,1,0:T(8,128)(2,1)} %param.35) | copy-start | bytes 6291460
  107.2 8.1 %collective-permute-start.7 = (bf16[16,64,128]{2,1,0:T(8,128)(2,1)S(1)}, bf16[16,64,128]{2,1,0:T(8,128)(2,1)S(1)}, u32[]{:S(2)}, u32[]{:S(2)}) collective-permute-start(bf16[16,64,128]{2,1,0:T(8,128)(2,1)S(1)} %all-to-all-done.3), channel_id=1, source_target_pairs={{0,1},{1,0},{2,3},{3,2},{4,5},{5,4},{6,7},{7,6},{8,9},{9,8},{10,11... | collective-permute-start | bytes 786440 | tf_op jit(solution)/shard_map/ppermute | solution.py:36
  119.9 28.3 %all-to-all-start.4 = ((bf16[32,2,2048]{2,1,0:T(2,128)(2,1)}), bf16[32,2,2048]{2,1,0:T(2,128)(2,1)S(1)}, u32[]{:S(2)}, u32[]{:S(2)}) async-start(bf16[32,2,2048]{2,1,0:T(2,128)(2,1)} %reshape.180), calls=%async_computation.4 | async-start | bytes 524288 | tf_op jit(solution)/shard_map/all_to_all | solution.py:314
  126.1 6.2 %copy-start.18 = (s32[4,4]{1,0:T(4,128)S(1)}, s32[4,4]{1,0:T(4,128)}, u32[]{:S(2)}) copy-start(s32[4,4]{1,0:T(4,128)} %param.33) | copy-start | bytes 196
  126.1 22.9 %copy-start.19 = (f32[4,4]{1,0:T(4,128)S(1)}, f32[4,4]{1,0:T(4,128)}, u32[]{:S(2)}) copy-start(f32[4,4]{1,0:T(4,128)} %param.34) | copy-start | bytes 196

commit v4 on v3

--- a/solution.py
+++ b/solution.py
@@ -9,6 +9,12 @@
 f32, bf16 = jnp.float32, jnp.bfloat16
 lanes = 128
 whole = pl.BlockSpec(memory_space=pltpu.VMEM)
+hbm = pl.BlockSpec(memory_space=pltpu.HBM)
+scalar = pl.BlockSpec(memory_space=pltpu.SMEM)
+
+
+def in_hbm(array):
+    return pltpu.with_memory_space_constraint(array, pltpu.HBM)
 
 
 def scaled_norm(entries, gain):
@@ -64,23 +70,29 @@
         gain_rows[rows, :] = jnp.broadcast_to(head_gain[chip : chip + 1, :], (seqs, lanes))
 
 
-def gather_tables(core, tables, out):
+def place_tables(core, tables):
     start = 0
     for mine, theirs in zip(tables[::2], tables[1::2]):
         count = mine.shape[0]
-        own = pl.multiple_of(start + core[0] * count, count)
-        other = pl.multiple_of(start + (1 - core[0]) * count, count)
-        out[pl.ds(own, count), :] = mine[...]
-        out[pl.ds(other, count), :] = theirs[...]
+        yield mine, pl.ds(pl.multiple_of(start + core[0] * count, count), count)
+        yield theirs, pl.ds(pl.multiple_of(start + (1 - core[0]) * count, count), count)
         start += 2 * count
 
 
-def project_kernel(core, blocks, gain, routing, *refs):
-    tables, (out, table, rows) = refs[:-3], refs[-3:]
+def project_kernel(core, blocks, routing, norm_gain, *refs):
+    tables, (out, table, rows, gain, arrived) = refs[:-5], refs[-5:]
     chips, seqs = blocks.shape[:2]
-    gather_tables(core, tables, table)
+    copies = [
+        pltpu.make_async_copy(source, table.at[where], arrived.at[i])
+        for i, (source, where) in enumerate(place_tables(core, tables))
+    ]
+    copies.append(pltpu.make_async_copy(norm_gain, gain, arrived.at[len(tables)]))
+    for copy in copies:
+        copy.start()
     for chip in range(chips):
         rows[chip * seqs : (chip + 1) * seqs, :] = blocks[chip].astype(f32)
+    for copy in copies:
+        copy.wait()
     normed = scaled_norm(rows[...], gain[...]).astype(bf16)
     columns = lax.dot_general(
         normed, table[...], (((1,), (1,)), ((), ())), preferred_element_type=f32
@@ -93,7 +105,8 @@
 
 def mix_kernel(core, blocks, mine, theirs, out, table, rows):
     chips, seqs = blocks.shape[:2]
-    gather_tables(core, (mine, theirs), table)
+    for source, where in place_tables(core, (mine, theirs)):
+        table[where, :] = source[...]
     for chip in range(chips):
         rows[chip * seqs : (chip + 1) * seqs, :] = blocks[chip].astype(f32)
     columns = lax.dot_general(
@@ -150,6 +163,80 @@
         tile = mixed[chip * seqs : (chip + 1) * seqs, :].astype(bf16)
         for copy in range(chips):
             out[copy, :, chip * lanes : (chip + 1) * lanes] = tile
+
+
+def pick_kernel(me, same_routed, other_routed, same_tokens, other_tokens, pick, picked, routed, rows):
+    chips, seqs = same_tokens.shape[:2]
+    half = chips * seqs
+    core = me[0] % 2
+    for chip in range(chips):
+        at = chip * seqs
+        routed[at : at + seqs, :] = same_routed[chip].astype(f32)
+        routed[half + at : half + at + seqs, :] = other_routed[chip].astype(f32)
+        rows[at : at + seqs, :] = same_tokens[chip].astype(f32)
+        rows[half + at : half + at + seqs, :] = other_tokens[chip].astype(f32)
+    choices = routed[...].T[:8]
+    valid = lax.broadcasted_iota(jnp.int32, choices.shape, 0) < seqs
+    hits = jnp.where(valid & (choices == me[0].astype(f32)), 1.0, 0.0)
+    named = jnp.broadcast_to(jnp.sum(hits, axis=0, keepdims=True), hits.shape)
+    lane = lax.broadcasted_iota(jnp.int32, hits.shape, 1)
+    slot = jnp.zeros(hits.shape, f32)
+    for back in range(1, seqs):
+        slot = slot + jnp.where(lane % seqs >= back, pltpu.roll(named, back, 1), 0.0)
+    source = 2 * (lane % half // seqs) + jnp.where(lane < half, core, 1 - core)
+    place = jnp.where(named > 0.0, 2 * source + slot.astype(jnp.int32), -1)
+    index = lax.broadcasted_iota(jnp.int32, pick.shape, 0)
+    slots = 4 * chips
+    mine = lax.broadcasted_iota(jnp.int32, pick.shape, 1) + slots - me[0] // 2 * seqs
+    wanted = jnp.where(index < slots, jnp.broadcast_to(place[:1], pick.shape), mine)
+    chosen = jnp.where(wanted == index, 1.0, 0.0).astype(bf16)
+    pick[...] = chosen
+    picked[...] = jnp.dot(chosen, rows[...].astype(bf16), preferred_element_type=f32).astype(bf16)
+
+
+def expert_kernel(pick, tokens, same, other, gain, gate, lift, down, out, own, branch, *refs):
+    gate_table, lift_table, down_table, arrived = refs
+    copies = [
+        pltpu.make_async_copy(source.at[0], target, arrived.at[i])
+        for i, (source, target) in enumerate(
+            ((gate, gate_table), (lift, lift_table), (down, down_table))
+        )
+    ]
+    for copy in copies:
+        copy.start()
+    chips, rows = same.shape[:2]
+    for chip in range(chips):
+        columns = slice(chip * lanes, (chip + 1) * lanes)
+        branch[:rows, columns] = same[chip]
+        branch[rows:, columns] = other[chip]
+    added = jnp.dot(pick[...], branch[...], preferred_element_type=f32)
+    residual = (tokens[...].astype(f32) + added).astype(bf16)
+    devices, capacity = out.shape[:2]
+    slots = devices * capacity
+    own[...] = residual[slots:][: own.shape[0]]
+    expert_in = scaled_norm(residual[:slots].astype(f32), gain[...]).astype(bf16)
+    copies[0].wait()
+    gate_value = jnp.dot(expert_in, gate_table[...], preferred_element_type=f32)
+    copies[1].wait()
+    lift_value = jnp.dot(expert_in, lift_table[...], preferred_element_type=f32)
+    hidden = (jax.nn.silu(gate_value) * lift_value).astype(bf16)
+    copies[2].wait()
+    results = jnp.dot(hidden, down_table[...], preferred_element_type=f32)
+    for device in range(devices):
+        out[device] = results[device * capacity : (device + 1) * capacity, :].astype(bf16)
+
+
+def combine_kernel(expert, slot, weights, returned, own, out):
+    seqs, choices = weights.shape
+    for seq in range(seqs):
+        total = jnp.zeros((1, out.shape[1]), f32)
+        for choice in range(choices):
+            pair = returned[expert[seq, choice]].astype(f32)
+            row = pair[:1]
+            for other in range(1, pair.shape[0]):
+                row = jnp.where(slot[seq, choice] == other, pair[other : other + 1], row)
+            total = total + (weights[seq, choice] * row).astype(bf16).astype(f32)
+        out[seq : seq + 1, :] = (own[seq : seq + 1, :].astype(f32) + total).astype(bf16)
 
 
 def body(
@@ -216,17 +303,21 @@
         (same_tokens, pairs, carried_rows, weight_rows, gain_rows, routing)
     )
 
-    scalar = pl.BlockSpec(memory_space=pltpu.SMEM)
     received = exchange(
         pl.pallas_call(
             project_kernel,
             out_shape=jax.ShapeDtypeStruct((chips, seq_rows, total + lanes), bf16),
-            in_specs=[scalar] + [whole] * (1 + len(pairs)),
+            in_specs=[scalar] + [whole] * 2 + [hbm] * (len(pairs) - 1),
             out_specs=whole,
-            scratch_shapes=[pltpu.VMEM((total, width), bf16), pltpu.VMEM((half_rows, width), f32)],
+            scratch_shapes=[
+                pltpu.VMEM((total, width), bf16),
+                pltpu.VMEM((half_rows, width), f32),
+                pltpu.VMEM((1, width), f32),
+                pltpu.SemaphoreType.DMA((len(pairs) - 1,)),
+            ],
             compiler_params=pltpu.CompilerParams(vmem_limit_bytes=8 << 20),
             name="project",
-        )(core[None], same_tokens, norm_gain[None], routing, *pairs[:-2])
+        )(core[None], same_tokens, routing, *map(in_hbm, [norm_gain[None]] + pairs[:-2]))
     )
     same_mixed = exchange(
         pl.pallas_call(
@@ -263,67 +354,77 @@
         + (written[:, :, None] * key_heads)[:, :, :, None] * value_heads[:, :, None, :]
     )
 
-    same_branch = exchange(
-        pl.pallas_call(
-            mix_kernel,
-            out_shape=jax.ShapeDtypeStruct((chips, half_rows, lanes), bf16),
-            in_specs=[scalar] + [whole] * 3,
-            out_specs=whole,
-            scratch_shapes=[pltpu.VMEM((lanes, width), bf16), pltpu.VMEM((half_rows, width), f32)],
-            compiler_params=pltpu.CompilerParams(vmem_limit_bytes=4 << 20),
-            name="mix",
-        )(core[None], same_mixed, *pairs[-2:])
-    )
-    other_branch = partner(same_branch)
-    other_tokens = partner(same_tokens)
-
-    same_tokens = same_tokens.reshape(half_rows, width)
-    other_tokens = other_tokens.reshape(half_rows, width)
+    columns = pl.pallas_call(
+        mix_kernel,
+        out_shape=jax.ShapeDtypeStruct((chips, half_rows, lanes), bf16),
+        in_specs=[scalar] + [whole] * 3,
+        out_specs=whole,
+        scratch_shapes=[pltpu.VMEM((lanes, width), bf16), pltpu.VMEM((half_rows, width), f32)],
+        compiler_params=pltpu.CompilerParams(vmem_limit_bytes=4 << 20),
+        name="mix",
+    )(core[None], same_mixed, *pairs[-2:])
+    same_branch = exchange(columns)
+    slots = axis_size * capacity
     same_routed = received[:, :, total:]
-    other_routed = partner(same_routed).reshape(half_rows, lanes)[:, :choices]
-    same_routed = same_routed.reshape(half_rows, lanes)[:, :choices]
-    same_named = jnp.any(same_routed == me.astype(bf16), axis=1).astype(jnp.int32)
-    other_named = jnp.any(other_routed == me.astype(bf16), axis=1).astype(jnp.int32)
-    named = jnp.stack([same_named, other_named]).reshape(2, chips, seq_rows)
-    slot = jnp.cumsum(named, axis=2) - named
-    source = 2 * jnp.arange(chips)[None, :, None] + jnp.stack([core, 1 - core])[:, None, None]
-    place = jnp.where(named > 0, source * capacity + slot, -1).reshape(2 * half_rows)
-    slots = axis_size * capacity
-    pick = place[None, :] == jnp.arange(slots)[:, None]
-    own = ((me // 2) * seq_rows + jnp.arange(seq_rows))[:, None] == jnp.arange(2 * half_rows)[None, :]
-    pick = jnp.concatenate([pick, own], axis=0).astype(bf16)
-    branch_rows = jnp.concatenate(
-        [b.transpose(1, 0, 2).reshape(half_rows, width) for b in (same_branch, other_branch)], axis=0
-    )
-    token_rows = jnp.concatenate([same_tokens, other_tokens], axis=0)
-    branch = jnp.dot(pick, branch_rows, preferred_element_type=f32)
-    picked_tokens = jnp.dot(pick, token_rows, preferred_element_type=f32)
-    residual = (picked_tokens + branch).astype(bf16)
-    own_residual = residual[slots:]
-    expert_in = scaled_norm(residual[:slots].astype(f32), expert_norm).astype(bf16)
-    hidden = (
-        jax.nn.silu(jnp.dot(expert_in, expert_gate[0], preferred_element_type=f32))
-        * jnp.dot(expert_in, expert_lift[0], preferred_element_type=f32)
-    ).astype(bf16)
-    results = (
-        jnp.dot(hidden, expert_down[0], preferred_element_type=f32)
-        .astype(bf16)
-        .reshape(axis_size, capacity, width)
+    pick, picked_tokens = pl.pallas_call(
+        pick_kernel,
+        out_shape=(
+            jax.ShapeDtypeStruct((slots + 16, 2 * half_rows), bf16),
+            jax.ShapeDtypeStruct((slots + 16, width), bf16),
+        ),
+        in_specs=[scalar] + [whole] * 4,
+        out_specs=(whole, whole),
+        scratch_shapes=[
+            pltpu.VMEM((2 * half_rows, lanes), f32),
+            pltpu.VMEM((2 * half_rows, width), f32),
+        ],
+        compiler_params=pltpu.CompilerParams(vmem_limit_bytes=8 << 20),
+        name="pick",
+    )(me[None], same_routed, partner(same_routed), same_tokens, partner(same_tokens))
+    picked_tokens, pick, same_branch = lax.optimization_barrier((picked_tokens, pick, same_branch))
+    results, own_residual = pl.pallas_call(
+        expert_kernel,
+        out_shape=(
+            jax.ShapeDtypeStruct((axis_size, capacity, width), bf16),
+            jax.ShapeDtypeStruct((seq_rows, width), bf16),
+        ),
+        in_specs=[whole] * 5 + [hbm] * 3,
+        out_specs=(whole, whole),
+        scratch_shapes=[
+            pltpu.VMEM((2 * half_rows, width), bf16),
+            pltpu.VMEM(expert_gate.shape[1:], bf16),
+            pltpu.VMEM(expert_lift.shape[1:], bf16),
+            pltpu.VMEM(expert_down.shape[1:], bf16),
+            pltpu.SemaphoreType.DMA((3,)),
+        ],
+        compiler_params=pltpu.CompilerParams(vmem_limit_bytes=24 << 20),
+        name="experts",
+    )(
+        pick,
+        picked_tokens,
+        same_branch,
+        partner(same_branch),
+        expert_norm[None],
+        *map(in_hbm, (expert_gate, expert_lift, expert_down)),
     )
     routed_experts, results = lax.optimization_barrier((routed_experts, results))
     returned = lax.all_to_all(results, "ep", split_axis=0, concat_axis=0, tiled=True)
-    expert_ids = jnp.arange(axis_size, dtype=jnp.int32)
-    chosen = (routed_experts[:, :, None] == expert_ids[None, None, :]).astype(jnp.int32)
-    present = jnp.sum(chosen, axis=1)
-    before = jnp.cumsum(present, axis=0) - present
-    slot_index = jnp.sum(chosen * before[:, None, :], axis=2)
-    picked = returned.reshape(slots, width)[routed_experts * capacity + slot_index]
-    weighted = lax.optimization_barrier(
-        (route_weights[:, :, None] * picked.astype(f32)).astype(bf16)
-    )
-    expert_sum = jnp.sum(weighted.astype(f32), axis=1)
-    layer_out = (own_residual.astype(f32) + expert_sum).astype(bf16)
+    earlier = jnp.arange(seq_rows)[:, None] > jnp.arange(seq_rows)[None, :]
+    same = routed_experts[:, :, None, None] == routed_experts[None, None, :, :]
+    slot_index = jnp.sum(
+        (same & earlier[:, None, :, None]).astype(jnp.int32), axis=(2, 3), dtype=jnp.int32
+    )
+    layer_out = pl.pallas_call(
+        combine_kernel,
+        out_shape=jax.ShapeDtypeStruct((seq_rows, width), bf16),
+        in_specs=[scalar] * 3 + [whole] * 2,
+        out_specs=whole,
+        compiler_params=pltpu.CompilerParams(vmem_limit_bytes=4 << 20),
+        name="combine",
+    )(routed_experts, slot_index, route_weights, returned, own_residual)
     return (layer_out, new_memory, new_max)
+
+
 def solution(mesh):
     return jax.shard_map(
         body,

time: 151 us -> 144 us (0.954)
  blocking collectives: 0 us -> 37.3 us
  waiting for transfers between devices: 52.1 us -> 31.1 us
  starting transfers between devices: 60.3 us -> 45.5 us
  local copies, waits for them, and re-layouts: 15.3 us -> 6.59 us
  Pallas kernels: 7.95 us -> 14.2 us
  matrix products: 3.54 us -> 0 us
  other arithmetic: 9.59 us -> 7.51 us
    all_to_all x0 -> x2, blocking collectives: none -> 37.3 us  [exchange(): lax.all_to_all(blocks, 'ep', split_axis=0, concat_axis=0, tiled=True, axi...]
    all_to_all x4 -> x2, waiting for transfers between devices: 35.5 us -> 13.6 us  [exchange(): lax.all_to_all(blocks, 'ep', split_axis=0, concat_axis=0, tiled=True, axi...]
    all_to_all x4 -> x2, starting transfers between devices: 42.8 us -> 28.1 us  [exchange(): lax.all_to_all(blocks, 'ep', split_axis=0, concat_axis=0, tiled=True, axi...]
    pallas_call x0 -> x3, Pallas kernels: none -> 6.24 us  [the longest x1 4.38 us: body(): pl.pallas_call(expert_kernel, out_shape=(jax.ShapeDtypeStruct((axis_size,...]
    unnamed x40 -> x30, local copies, waits for them, and re-layouts: 10.1 us -> 4.91 us
    dot_general x4 -> x0, matrix products: 3.54 us -> none  [the longest x1 2.55 us: body(): jnp.dot(hidden, expert_down[0], preferred_element_type=f32).astype(bf16)]
    reshape x6 -> x0, local copies, waits for them, and re-layouts: 2.12 us -> none  [the longest x1 1.01 us: body(): other_tokens = other_tokens.reshape(half_rows, width)]
  transfers between devices with their start and end apart: 13 -> 11, of which waited for: 6 -> 5; matrix products, arithmetic and copies ran while one was open for 7% -> 5% of each run, Pallas kernels for 1% -> 1%
where the time goes in v4:
time: 144 us; the launch traced here: 143 us
  starting transfers between devices  45.5 us (32%)
  blocking collectives  37.3 us (26%)
  waiting for transfers between devices  31.1 us (22%)
  Pallas kernels  14.2 us (10%)
  other arithmetic  7.51 us (5%)
  local copies, waits for them, and re-layouts  6.59 us (5%)
    all_to_all x2, blocking collectives, exchange(): lax.all_to_all(blocks, 'ep', split_axis=0, concat_axis=0, tiled=True, axi...  37.3 us
    all_to_all x2, starting transfers between devices, exchange(): lax.all_to_all(blocks, 'ep', split_axis=0, concat_axis=0, tiled=True, axi...  28.1 us
    all_to_all x1, waiting for transfers between devices, body(): lax.all_to_all(results, 'ep', split_axis=0, concat_axis=0, tiled=True)  15.2 us
    all_to_all x2, waiting for transfers between devices, exchange(): lax.all_to_all(blocks, 'ep', split_axis=0, concat_axis=0, tiled=True, axi...  13.6 us
    ppermute x8, starting transfers between devices, partner(): lax.ppermute(block, 'ep', [(i, i ^ 1) for i in range(lax.axis_size('ep'))])  11.2 us
    all_to_all x1, starting transfers between devices, body(): lax.all_to_all(results, 'ep', split_axis=0, concat_axis=0, tiled=True)  6.27 us
    add x1, other arithmetic, body(): carried[:, :, None, None] * memory_state  6.21 us
    unnamed x30, local copies, waits for them, and re-layouts  4.91 us
  transfers between devices with their start and end apart: 11, of which 5 were waited for; matrix products, arithmetic and copies ran while one was open for 5% of the time, Pallas kernels for 1%

profile of v4, /device:TPU:69, one launch (start us, length us, event | category | flops | bytes accessed | tf_op | source)
XLA Modules:
  0.0 143.0 jit_solution(8550944057827527275)
XLA Ops:
  0.6 0.0 copy-start
  0.6 0.0 copy-start.7
  0.7 1.6 %broadcast_in_dim.14 = bf16[16,4,2048]{2,1,0:T(4,128)(2,1)} broadcast(bf16[4,2048]{1,0:T(4,128)(2,1)} %refs_0_.1), dimensions={1,2} | broadcast | bytes 278528 | tf_op jit(solution)/shard_map/broadcast_in_dim | solution.py:38
  2.2 17.6 %all-to-all-start = ((bf16[16,4,2048]{2,1,0:T(4,128)(2,1)}), bf16[16,4,2048]{2,1,0:T(4,128)(2,1)S(1)}, u32[]{:S(2)}, u32[]{:S(2)}) async-start(bf16[16,4,2048]{2,1,0:T(4,128)(2,1)} %broadcast_in_dim.14), calls=%async_computation | async-start | bytes 524288 | tf_op jit(solution)/shard_map/all_to_all | solution.py:26
  19.8 1.0 collective-permute-start.2
  20.8 0.1 collective-permute-start.3
  20.9 0.4 collective-permute-start.4
  21.3 0.1 collective-permute-start
  21.5 0.4 collective-permute-start.1
  21.8 0.7 convert_element_type.34
  22.5 0.7 copy-done.1
  23.2 0.7 copy-done.2
  23.9 0.7 copy-done.4
  24.6 0.7 copy-done.5
  25.4 0.7 copy-done.6
  26.1 0.7 copy-done.9
  26.7 0.7 copy-done.10
  27.4 0.9 gates.1
  28.3 0.0 collective-permute-done.refs_1_
  28.3 0.0 collective-permute-done.1.refs_3_
  28.3 0.0 copy-start.14
  28.3 0.0 collective-permute-done.2.refs_5_
  28.3 0.0 collective-permute-done.3.refs_7_
  28.3 0.0 collective-permute-done.4.theirs
  28.3 5.0 %all-to-all-done.blocks.same_tokens = bf16[16,4,2048]{2,1,0:T(4,128)(2,1)S(1)} async-done(((bf16[16,4,2048]{2,1,0:T(4,128)(2,1)}), bf16[16,4,2048]{2,1,0:T(4,128)(2,1)S(1)}, u32[]{:S(2)}, u32[]{:S(2)}) %all-to-all-start) | async-done | bytes 262176 | tf_op jit(solution)/shard_map/all_to_all | solution.py:26
  33.4 2.2 %project.1 = bf16[16,4,512]{2,1,0:T(4,128)(2,1)S(1)} custom-call(s32[1]{0:T(128)} %bitcast.1.core, bf16[16,4,2048]{2,1,0:T(4,128)(2,1)S(1)} %all-to-all-done.blocks.same_tokens, bf16[4,128]{1,0:T(4,128)(2,1)S(1)} %pad.4.routing, f32[1,2048]{1,0:T(1,128)} %bitcast.19, bf16[32,2048]{1,0:T(8,128)(2,1)} %bitcast.31, bf16[32,2048]{1,0:T(8,128)(2,1)} %copy-done.13, ...), custom_call_target="tpu_custom_call" | custom-call | tf_op jit(solution)/shard_map/project/pallas_call | solution.py:307
  35.6 21.7 %all_to_all.25.received = bf16[16,4,512]{2,1,0:T(4,128)(2,1)S(1)} all-to-all(bf16[16,4,512]{2,1,0:T(4,128)(2,1)S(1)} %project.1), channel_id=1, replica_groups={{0,2,4,6,8,10,12,14,16,18,20,22,24,26,28,30},{1,3,5,7,9,11,13,15,17,19,..., dimensions={0} | all-to-all | bytes 131072 | tf_op jit(solution)/shard_map/all_to_all | solution.py:26
  57.3 3.9 %readout.1 = bf16[16,4,2048]{2,1,0:T(4,128)(2,1)S(1)} custom-call(f32[4,4,256,512]{3,2,1,0:T(8,128)} %state.1, bf16[16,4,512]{2,1,0:T(4,128)(2,1)S(1)} %all_to_all.25.received, f32[64,128]{1,0:T(8,128)S(1)} %get-tuple-element.48.carried, f32[64,128]{1,0:T(8,128)S(1)} %get-tuple-element.49.weight, f32[64,128]{1,0:T(8,128)S(1)} %get-tuple-element.50.gain), custom_call_target="tpu_custom_call" | custom-call | tf_op jit(solution)/shard_map/readout/pallas_call | solution.py:323
  61.1 15.6 %all_to_all.26.blocks = bf16[16,4,2048]{2,1,0:T(4,128)(2,1)S(1)} all-to-all(bf16[16,4,2048]{2,1,0:T(4,128)(2,1)S(1)} %readout.1), channel_id=1, replica_groups={{0,2,4,6,8,10,12,14,16,18,20,22,24,26,28,30},{1,3,5,7,9,11,13,15,17,19,..., dimensions={0} | all-to-all | bytes 524288 | tf_op jit(solution)/shard_map/all_to_all | solution.py:26
  76.7 1.1 mix.1
  77.8 10.5 %all-to-all-start.3 = ((bf16[16,64,128]{2,1,0:T(8,128)(2,1)}), bf16[16,64,128]{2,1,0:T(8,128)(2,1)S(1)}, u32[]{:S(2)}, u32[]{:S(2)}) async-start(bf16[16,64,128]{2,1,0:T(8,128)(2,1)} %mix.1), calls=%async_computation.3 | async-start | bytes 524288 | tf_op jit(solution)/shard_map/all_to_all | solution.py:26
  88.3 2.2 %collective-permute-start.6 = (bf16[16,4,2048]{2,1,0:T(4,128)(2,1)S(1)}, bf16[16,4,2048]{2,1,0:T(4,128)(2,1)S(1)}, u32[]{:S(2)}, u32[]{:S(2)}) collective-permute-start(bf16[16,4,2048]{2,1,0:T(4,128)(2,1)S(1)} %all-to-all-done.blocks.same_tokens), channel_id=1, source_target_pairs={{0,1},{1,0},{2,3},{3,2},{4,5},{5,4},{6,7},{7,6},{8,9},{9,8},{10,11... | collective-permute-start | bytes 786440 | tf_op jit(solution)/shard_map/ppermute | solution.py:42
  90.5 0.1 collective-permute-start.5
  90.7 1.2 collective-permute-done.5.other_routed
  91.8 0.0 collective-permute-done.6.other_tokens
  91.8 0.4 pick.1
  92.3 8.5 %all-to-all-done.3.same = bf16[16,64,128]{2,1,0:T(8,128)(2,1)S(1)} async-done(((bf16[16,64,128]{2,1,0:T(8,128)(2,1)}), bf16[16,64,128]{2,1,0:T(8,128)(2,1)S(1)}, u32[]{:S(2)}, u32[]{:S(2)}) %all-to-all-start.3) | async-done | bytes 262176 | tf_op jit(solution)/shard_map/all_to_all | solution.py:26
  100.8 6.8 %collective-permute-start.7 = (bf16[16,64,128]{2,1,0:T(8,128)(2,1)S(1)}, bf16[16,64,128]{2,1,0:T(8,128)(2,1)S(1)}, u32[]{:S(2)}, u32[]{:S(2)}) collective-permute-start(bf16[16,64,128]{2,1,0:T(8,128)(2,1)S(1)} %all-to-all-done.3.same), channel_id=1, source_target_pairs={{0,1},{1,0},{2,3},{3,2},{4,5},{5,4},{6,7},{7,6},{8,9},{9,8},{10,11... | collective-permute-start | bytes 786440 | tf_op jit(solution)/shard_map/ppermute | solution.py:42
  107.6 1.2 collective-permute-done.7.other
  108.7 4.4 %experts.1 = (bf16[32,2,2048]{2,1,0:T(2,128)(2,1)}, bf16[4,2048]{1,0:T(4,128)(2,1)S(1)}) custom-call(bf16[80,128]{1,0:T(8,128)(2,1)S(1)} %get-tuple-element.53.pick, bf16[80,2048]{1,0:T(8,128)(2,1)S(1)} %get-tuple-element.54.tokens, bf16[16,64,128]{2,1,0:T(8,128)(2,1)S(1)} %all-to-all-done.3.same, bf16[16,64,128]{2,1,0:T(8,128)(2,1)S(1)} %collective-permute-done.7.other, ...), custom_call_target="tpu_custom_call" | custom-call | tf_op jit(solution)/shard_map/experts/pallas_call | solution.py:385
  113.1 6.3 %all-to-all-start.4 = ((bf16[32,2,2048]{2,1,0:T(2,128)(2,1)}), bf16[32,2,2048]{2,1,0:T(2,128)(2,1)S(1)}, u32[]{:S(2)}, u32[]{:S(2)}) async-start(bf16[32,2,2048]{2,1,0:T(2,128)(2,1)} %get-tuple-element.58), calls=%async_computation.4 | async-start | bytes 524288 | tf_op jit(solution)/shard_map/all_to_all | solution.py:411
  119.4 0.1 convert_bitcast_fusion.1
  119.5 0.1 reshape.44
  119.6 0.1 broadcast_multiply_fusion
  119.7 6.2 %multiply_add_fusion = f32[4,4,256,512]{3,2,1,0:T(8,128)} fusion(f32[4,4,256,512]{3,2,1,0:T(8,128)} %state.1, f32[4,4,512]{2,1,0:T(4,128)S(1)} %reshape.45, f32[4,4,256]{2,1,0:T(4,128)S(1)} %broadcast_multiply_fusion, f32[4,4]{1,0:T(4,128)S(1)} %get-tuple-element.60), kind=kLoop, calls=%fused_computation | loop fusion | flops 6291456 | bytes 16826432 | tf_op jit(solution)/shard_map/add | solution.py:353
  125.9 0.4 convert_reduce_fusion.slot
  126.3 15.2 %all-to-all-done.4.returned = bf16[32,2,2048]{2,1,0:T(2,128)(2,1)S(1)} async-done(((bf16[32,2,2048]{2,1,0:T(2,128)(2,1)}), bf16[32,2,2048]{2,1,0:T(2,128)(2,1)S(1)}, u32[]{:S(2)}, u32[]{:S(2)}) %all-to-all-start.4) | async-done | bytes 262176 | tf_op jit(solution)/shard_map/all_to_all | solution.py:411
  141.5 1.4 %combine.1 = bf16[4,2048]{1,0:T(4,128)(2,1)} custom-call(s32[4,4]{1,0:T(4,128)S(1)} %copy-done.3, s32[4,4]{1,0:T(4,128)S(1)} %convert_reduce_fusion.slot, f32[4,4]{1,0:T(4,128)S(1)} %copy-done.8, bf16[32,2,2048]{2,1,0:T(2,128)(2,1)S(1)} %all-to-all-done.4.returned, bf16[4,2048]{1,0:T(4,128)(2,1)S(1)} %get-tuple-element.59.own), custom_call_target="tpu_custom_call" | custom-call | tf_op jit(solution)/shard_map/combine/pallas_call | solution.py:417
  (26 shorter events, 0.1 us)
Async XLA Ops:
  0.6 76.1 %copy-start = (bf16[2048,64]{0,1:T(8,128)(2,1)S(1)}, bf16[2048,64]{0,1:T(8,128)(2,1)}, u32[]{:S(2)}) copy-start(bf16[2048,64]{0,1:T(8,128)(2,1)} %param.31) | copy-start | bytes 786436
  0.6 108.1 %copy-start.7 = (f32[2048]{0:T(1024)S(1)}, f32[2048]{0:T(1024)}, u32[]{:S(2)}) copy-start(f32[2048]{0:T(1024)} %param.32) | copy-start | bytes 24580
  2.2 31.1 %all-to-all-start = ((bf16[16,4,2048]{2,1,0:T(4,128)(2,1)}), bf16[16,4,2048]{2,1,0:T(4,128)(2,1)S(1)}, u32[]{:S(2)}, u32[]{:S(2)}) async-start(bf16[16,4,2048]{2,1,0:T(4,128)(2,1)} %broadcast_in_dim.14), calls=%async_computation | async-start | bytes 524288 | tf_op jit(solution)/shard_map/all_to_all | solution.py:26
  19.8 8.5 %collective-permute-start.2 = (bf16[64,2048]{1,0:T(8,128)(2,1)}, bf16[64,2048]{1,0:T(8,128)(2,1)S(1)}, u32[]{:S(2)}, u32[]{:S(2)}) collective-permute-start(bf16[64,2048]{1,0:T(8,128)(2,1)} %bitcast.26), channel_id=1, source_target_pairs={{0,1},{1,0},{2,3},{3,2},{4,5},{5,4},{6,7},{7,6},{8,9},{9,8},{10,11... | collective-permute-start | bytes 786440 | tf_op jit(solution)/shard_map/ppermute | solution.py:42
  20.8 7.5 %collective-permute-start.3 = (bf16[64,2048]{1,0:T(8,128)(2,1)}, bf16[64,2048]{1,0:T(8,128)(2,1)S(1)}, u32[]{:S(2)}, u32[]{:S(2)}) collective-permute-start(bf16[64,2048]{1,0:T(8,128)(2,1)} %bitcast.28), channel_id=1, source_target_pairs={{0,1},{1,0},{2,3},{3,2},{4,5},{5,4},{6,7},{7,6},{8,9},{9,8},{10,11... | collective-permute-start | bytes 786440 | tf_op jit(solution)/shard_map/ppermute | solution.py:42
  20.9 7.4 %collective-permute-start.4 = (bf16[64,2048]{1,0:T(8,128)(2,1)}, bf16[64,2048]{1,0:T(8,128)(2,1)S(1)}, u32[]{:S(2)}, u32[]{:S(2)}) collective-permute-start(bf16[64,2048]{1,0:T(8,128)(2,1)} %bitcast.17), channel_id=1, source_target_pairs={{0,1},{1,0},{2,3},{3,2},{4,5},{5,4},{6,7},{7,6},{8,9},{9,8},{10,11... | collective-permute-start | bytes 786440 | tf_op jit(solution)/shard_map/ppermute | solution.py:42
  21.3 7.0 %collective-permute-start = (bf16[32,2048]{1,0:T(8,128)(2,1)}, bf16[32,2048]{1,0:T(8,128)(2,1)S(1)}, u32[]{:S(2)}, u32[]{:S(2)}) collective-permute-start(bf16[32,2048]{1,0:T(8,128)(2,1)} %bitcast.30), channel_id=1, source_target_pairs={{0,1},{1,0},{2,3},{3,2},{4,5},{5,4},{6,7},{7,6},{8,9},{9,8},{10,11... | collective-permute-start | bytes 393224 | tf_op jit(solution)/shard_map/ppermute | solution.py:42
  21.5 6.8 %collective-permute-start.1 = (bf16[32,2048]{1,0:T(8,128)(2,1)}, bf16[32,2048]{1,0:T(8,128)(2,1)S(1)}, u32[]{:S(2)}, u32[]{:S(2)}) collective-permute-start(bf16[32,2048]{1,0:T(8,128)(2,1)} %bitcast.32), channel_id=1, source_target_pairs={{0,1},{1,0},{2,3},{3,2},{4,5},{5,4},{6,7},{7,6},{8,9},{9,8},{10,11... | collective-permute-start | bytes 393224 | tf_op jit(solution)/shard_map/ppermute | solution.py:42
  22.5 0.7 copy-start.1
  23.2 0.7 copy-start.2
  23.9 0.7 copy-start.4
  24.6 0.7 copy-start.5
  25.4 0.7 copy-start.6
  26.1 0.7 copy-start.9
  26.7 0.7 copy-start.10
  28.3 5.1 %copy-start.13 = (bf16[32,2048]{1,0:T(8,128)(2,1)}, bf16[32,2048]{1,0:T(8,128)(2,1)S(1)}, u32[]{:S(2)}) copy-start(bf16[32,2048]{1,0:T(8,128)(2,1)S(1)} %collective-permute-done.refs_1_) | copy-start | bytes 393220
  28.3 5.1 %copy-start.14 = (bf16[32,2048]{1,0:T(8,128)(2,1)}, bf16[32,2048]{1,0:T(8,128)(2,1)S(1)}, u32[]{:S(2)}) copy-start(bf16[32,2048]{1,0:T(8,128)(2,1)S(1)} %collective-permute-done.1.refs_3_) | copy-start | bytes 393220
  28.3 5.1 %copy-start.11 = (bf16[64,2048]{1,0:T(8,128)(2,1)}, bf16[64,2048]{1,0:T(8,128)(2,1)S(1)}, u32[]{:S(2)}) copy-start(bf16[64,2048]{1,0:T(8,128)(2,1)S(1)} %collective-permute-done.2.refs_5_) | copy-start | bytes 786436
  28.3 5.1 %copy-start.12 = (bf16[64,2048]{1,0:T(8,128)(2,1)}, bf16[64,2048]{1,0:T(8,128)(2,1)S(1)}, u32[]{:S(2)}) copy-start(bf16[64,2048]{1,0:T(8,128)(2,1)S(1)} %collective-permute-done.3.refs_7_) | copy-start | bytes 786436
  77.8 23.0 %all-to-all-start.3 = ((bf16[16,64,128]{2,1,0:T(8,128)(2,1)}), bf16[16,64,128]{2,1,0:T(8,128)(2,1)S(1)}, u32[]{:S(2)}, u32[]{:S(2)}) async-start(bf16[16,64,128]{2,1,0:T(8,128)(2,1)} %mix.1), calls=%async_computation.3 | async-start | bytes 524288 | tf_op jit(solution)/shard_map/all_to_all | solution.py:26
  88.3 3.5 %collective-permute-start.6 = (bf16[16,4,2048]{2,1,0:T(4,128)(2,1)S(1)}, bf16[16,4,2048]{2,1,0:T(4,128)(2,1)S(1)}, u32[]{:S(2)}, u32[]{:S(2)}) collective-permute-start(bf16[16,4,2048]{2,1,0:T(4,128)(2,1)S(1)} %all-to-all-done.blocks.same_tokens), channel_id=1, source_target_pairs={{0,1},{1,0},{2,3},{3,2},{4,5},{5,4},{6,7},{7,6},{8,9},{9,8},{10,11... | collective-permute-start | bytes 786440 | tf_op jit(solution)/shard_map/ppermute | solution.py:42
  90.5 1.3 collective-permute-start.5
  100.8 7.9 %collective-permute-start.7 = (bf16[16,64,128]{2,1,0:T(8,128)(2,1)S(1)}, bf16[16,64,128]{2,1,0:T(8,128)(2,1)S(1)}, u32[]{:S(2)}, u32[]{:S(2)}) collective-permute-start(bf16[16,64,128]{2,1,0:T(8,128)(2,1)S(1)} %all-to-all-done.3.same), channel_id=1, source_target_pairs={{0,1},{1,0},{2,3},{3,2},{4,5},{5,4},{6,7},{7,6},{8,9},{9,8},{10,11... | collective-permute-start | bytes 786440 | tf_op jit(solution)/shard_map/ppermute | solution.py:42
  113.1 28.4 %all-to-all-start.4 = ((bf16[32,2,2048]{2,1,0:T(2,128)(2,1)}), bf16[32,2,2048]{2,1,0:T(2,128)(2,1)S(1)}, u32[]{:S(2)}, u32[]{:S(2)}) async-start(bf16[32,2,2048]{2,1,0:T(2,128)(2,1)} %get-tuple-element.58), calls=%async_computation.4 | async-start | bytes 524288 | tf_op jit(solution)/shard_map/all_to_all | solution.py:411
  119.7 6.2 %copy-start.3 = (s32[4,4]{1,0:T(4,128)S(1)}, s32[4,4]{1,0:T(4,128)}, u32[]{:S(2)}) copy-start(s32[4,4]{1,0:T(4,128)} %expert) | copy-start | bytes 196
  119.7 21.8 %copy-start.8 = (f32[4,4]{1,0:T(4,128)S(1)}, f32[4,4]{1,0:T(4,128)}, u32[]{:S(2)}) copy-start(f32[4,4]{1,0:T(4,128)} %weights.1) | copy-start | bytes 196
